TPU v7x, 128 devices: a whole 4x4x4 slice. The times are simulated.
128 devices in a mesh: sp: 16 (over z, y), tp: 8 (over x, core).
Axes of the slice: x: 4, y: 4, z: 4, core: 2. Of those that a mesh axis runs over, the one named last changes fastest.
Arguments:
- layer_input: bfloat16 [16, 4096, 2048], P(None, ('sp', 'tp')), may hold values from -6 to 6
- input_gain: float32 [2048], replicated, may hold values from 0.5 to 1.5
- narrowing_matrix: bfloat16 [2048, 512], replicated, may hold values from -0.125 to 0.125
- rotary_down: bfloat16 [2048, 64], replicated, may hold values from -0.125 to 0.125
- summary_scaling: float32 [512], replicated, may hold values from 0.5 to 1.5
- lookup_widening: bfloat16 [512, 16, 128], P('tp'), may hold values from -0.25 to 0.25
- payload_widening: bfloat16 [512, 16, 128], P('tp'), may hold values from -0.25 to 0.25
- query_nope: bfloat16 [16, 16, 128], P('sp', 'tp'), may hold values from -6 to 6
- query_rotary: bfloat16 [16, 16, 64], P('sp', 'tp'), may hold values from -6 to 6
Outputs:
- stored_summaries: bfloat16 [16, 4096, 512], P('sp', None, 'tp')
- rotary_cache: bfloat16 [16, 4096, 64], P('sp', None, 'tp')
- first_read: bfloat16 [16, 16, 128], P('sp', 'tp')
All inputs are finite; a program needn't handle non-finite values.
Results may differ from a plain program's by a relative error of at most 0.02.
Values may be sent and summed in bfloat16 or wider, within the bound.
No kernel may reach another device: no remote copies, remote signals or barrier semaphores. Data moves between devices by JAX's collectives and lax.ppermute only.
A program may use at most 64 MiB of HBM per device.

v0:
```python
import jax
import jax.numpy as jnp
from jax import lax
from jax.experimental import pallas as pl
from jax.experimental.pallas import tpu as pltpu
from jax.sharding import Mesh
from jax.sharding import PartitionSpec as P

QK_ROPE = 64
PLAIN_MATCH_SPAN = 128
TP = ("x", "c")
SP_TP = ("sp", "x", "c")

norm_eps = 1e-06
rotary_base = 10000.0
F32 = jnp.float32
BF16 = jnp.bfloat16
LAST = (((1,), (1,)), ((), ()))


def frequencies():
    half = QK_ROPE // 2
    return 1.0 / rotary_base ** (jnp.arange(half, dtype=F32) * 2.0 / QK_ROPE)


def rotate(vector, position):
    half_width = vector.shape[-1] // 2
    angles = position * frequencies()
    first_half = vector[..., :half_width]
    second_half = vector[..., half_width:]
    return jnp.concatenate(
        [
            first_half * jnp.cos(angles) - second_half * jnp.sin(angles),
            second_half * jnp.cos(angles) + first_half * jnp.sin(angles),
        ],
        axis=-1,
    )


def place_queries_kernel(at_ref, mine_ref, partner_ref, out_ref):
    mine = mine_ref[...].astype(F32)
    partner = partner_ref[...].astype(F32)
    first = jnp.where(at_ref[1] == 0, mine, partner)
    second = jnp.where(at_ref[1] == 0, partner, mine)
    rows = jnp.concatenate([first, second] * 4, axis=0)
    row = lax.broadcasted_iota(jnp.int32, rows.shape, 0) // 4
    out_ref[...] = jnp.where(row == at_ref[0], rows, 0.0).astype(BF16)


def pack_payload_kernel(at_ref, own_ref, other_ref, *refs):
    outs, (own_f32, other_f32) = refs[:4], refs[4:]
    heads = own_ref.shape[1]
    own_f32[...] = own_ref[...].astype(F32).reshape(own_f32.shape)
    other_f32[...] = other_ref[...].astype(F32).reshape(other_f32.shape)
    for d, out_ref in enumerate(outs):
        first = 2 * (2 * ((at_ref[0] + d) % 4) + at_ref[1])
        for r, source in enumerate((own_f32, other_f32)):
            for h in range(2):
                rows = source[pl.ds(first + h, out_ref.shape[1], stride=heads), :]
                out_ref[r, :, h * 128 : (h + 1) * 128] = rows.astype(BF16)


def project_kernel(x_ref, gain_ref, w_ref, r_ref, scal_ref, cs_ref, out_ref):
    rows = x_ref.shape[0]
    step = 128
    gain = gain_ref[...]
    scal = scal_ref[...]
    seqs = step // 32
    cos = jnp.concatenate([cs_ref[0]] * seqs, axis=0)
    sin = jnp.concatenate([cs_ref[1]] * seqs, axis=0)
    for i in range(rows // step):
        x = x_ref[i * step : (i + 1) * step, :].astype(F32)
        mean = jnp.mean(x * x, axis=-1, keepdims=True)
        normed = (x * lax.rsqrt(mean + norm_eps) * gain).astype(BF16)
        lat = jnp.dot(normed, w_ref[...], preferred_element_type=F32).astype(BF16).astype(F32)
        rot = lax.dot_general(normed, r_ref[...], LAST, preferred_element_type=F32)
        rot = rot.astype(BF16).astype(F32)
        mean = jnp.mean(lat * lat, axis=-1, keepdims=True)
        lat = (lat * lax.rsqrt(mean + norm_eps) * scal).astype(BF16)
        swapped = jnp.concatenate([rot[:, 32:], rot[:, :32]], axis=1)
        rot = rot * cos + swapped * sin
        rot = jnp.concatenate([rot, jnp.zeros_like(rot)], axis=1).astype(BF16)
        for s in range(seqs):
            slot = out_ref.shape[0] - 1 - (i * seqs + s)
            out_ref[slot, :, 0:512] = lat[s * 32 : (s + 1) * 32]
            out_ref[slot, :, 512:640] = rot[s * 32 : (s + 1) * 32]


def attend_kernel(z_ref, a0_ref, a1_ref, t_ref, out_ref):
    order = range(z_ref.shape[0] - 1, -1, -1)
    lat = jnp.concatenate([z_ref[i, :, 0:512] for i in order], axis=0)
    rot = jnp.concatenate([z_ref[i, :, 512:640] for i in order], axis=0)
    absorbed = a0_ref[...] + a1_ref[...]
    scores = lax.dot_general(absorbed, lat, LAST, preferred_element_type=F32)
    scores = scores + lax.dot_general(t_ref[...], rot, LAST, preferred_element_type=F32)
    scores = scores * ((PLAIN_MATCH_SPAN + QK_ROPE) ** (-0.5))
    top = jnp.max(scores, axis=-1, keepdims=True).astype(BF16).astype(F32)
    weight = jnp.exp(scores - top)
    total = jnp.sum(weight, axis=-1, keepdims=True)
    context = jnp.dot(weight.astype(BF16), lat, preferred_element_type=F32)
    high = total.astype(BF16).astype(F32)
    low = total - high
    top = jnp.broadcast_to(top, context.shape)
    high = jnp.broadcast_to(high, context.shape)
    low = jnp.broadcast_to(low, context.shape)
    lat_t = lat.T
    rot_t = rot.astype(F32).T
    for t in range(out_ref.shape[0]):
        slot = out_ref.shape[0] - 1 - t
        out_ref[slot, 0:64, :] = lat_t[64 * t : 64 * (t + 1)]
        mine = slice(2 * t, 2 * t + 2)
        block = jnp.concatenate(
            [rot_t[8 * t : 8 * t + 8], context[mine], top[mine], high[mine], low[mine]], axis=0
        )
        out_ref[slot, 64:80, :] = block.astype(BF16)


def order_payload_kernel(at_ref, p0_ref, p1_ref, p2_ref, p3_ref, out_ref):
    for d, piece in enumerate((p0_ref, p1_ref, p2_ref, p3_ref)):
        chip = (at_ref[0] + 4 - d) % 4
        out_ref[2 * chip + at_ref[1]] = piece[0]
        out_ref[2 * chip + 1 - at_ref[1]] = piece[1]


def finish_kernel(y_ref, w_ref, st_ref, rt_ref, fr_ref):
    count = y_ref.shape[0]
    for q in range(4):
        for o in range(4):
            for j in range(2):
                lanes = slice((4 * q + o) * 32, (4 * q + o) * 32 + 32)
                tile = jnp.concatenate(
                    [y_ref[count - 1 - (4 * j + k), 0:80, lanes] for k in range(4)], axis=1
                )
                at = (4 * q + o) * 256 + j * 128
                st_ref[:, at : at + 128] = tile[0:64]
                rt_ref[:, at : at + 128] = tile[64:72]
    tails = [y_ref[t, 64:80, :].astype(F32)[8:16] for t in range(count)]
    tops = [v[2:4] for v in tails]
    peak = tops[0]
    for v in tops[1:]:
        peak = jnp.maximum(peak, v)
    number = jnp.zeros_like(peak)
    denominator = jnp.zeros_like(peak)
    for v, top in zip(tails, tops):
        scale = jnp.exp(top - peak)
        number = number + scale * v[0:2]
        denominator = denominator + scale * (v[4:6] + v[6:8])
    context = (number / denominator).astype(BF16)
    weight = w_ref[...].reshape(count * 64, 256)
    values = jnp.dot(context, weight, preferred_element_type=F32)
    values = jnp.concatenate([values[0:1, 0:128], values[1:2, 128:256]], axis=0)
    mean = jnp.mean(values * values, axis=-1, keepdims=True)
    fr_ref[...] = (values * lax.rsqrt(mean + norm_eps)).astype(BF16)


def exchange(array, sp, tp, over_sp):
    if over_sp:
        groups = [[s * tp + t for s in reversed(range(sp))] for t in range(tp)]
    else:
        groups = [[s * tp + t for t in reversed(range(tp))] for s in range(sp)]
    return lax.all_to_all(array, SP_TP, 0, 0, tiled=True, axis_index_groups=groups)


def call(kernel, out_shape, flops, moved, **kwargs):
    return pl.pallas_call(
        kernel,
        out_shape=out_shape,
        **kwargs,
        cost_estimate=pl.CostEstimate(flops=flops, bytes_accessed=moved, transcendentals=0),
        compiler_params=pltpu.CompilerParams(vmem_limit_bytes=32 * 1024 * 1024),
    )


def shards(
    layer_input,
    input_gain,
    narrowing_matrix,
    rotary_down,
    summary_scaling,
    lookup_widening,
    payload_widening,
    query_nope,
    query_rotary,
):
    seqs, pos_local, width = layer_input.shape
    tp = lax.axis_size(TP)
    sp = lax.axis_size("sp")
    block = lax.axis_index(SP_TP)
    shape = jax.ShapeDtypeStruct

    at = jnp.stack([lax.axis_index("x"), lax.axis_index("c")]).astype(jnp.int32)
    small = pl.BlockSpec(memory_space=pltpu.SMEM)
    whole = pl.BlockSpec(memory_space=pltpu.VMEM)
    outside = pl.BlockSpec(memory_space=pltpu.HBM)
    swap = [(0, 1), (1, 0)]
    lookup_other = lax.ppermute(lookup_widening, "c", swap)
    payload_other = lax.ppermute(payload_widening, "c", swap)
    mine = jnp.concatenate(
        [query_nope[0], query_rotary[0], jnp.zeros_like(query_rotary[0])], axis=1
    )
    partner = lax.ppermute(mine, "c", swap)
    query = call(
        place_queries_kernel,
        shape((2 * tp, 256), BF16),
        30_000_000_000,
        60_000_000,
        in_specs=[small, whole, whole],
    )(at, mine, partner)
    near, far = [(0, 1), (1, 0), (2, 3), (3, 2)], [(0, 3), (3, 0), (1, 2), (2, 1)]
    moved = lax.ppermute(query, "x", near)
    query = query + moved
    moved = lax.ppermute(query, "x", far)

    positions = (block * pos_local + jnp.arange(pos_local, dtype=jnp.int32)).astype(F32)
    angles = positions[:, None] * frequencies()[None, :]
    cos, sin = jnp.cos(angles), jnp.sin(angles)
    table = jnp.stack(
        [jnp.concatenate([cos, cos], axis=1), jnp.concatenate([-sin, sin], axis=1)]
    )
    sent = call(
        project_kernel,
        shape((seqs, pos_local, 640), BF16),
        1_300_000_000,
        5_000_000,
    )(
        layer_input.reshape(seqs * pos_local, width),
        input_gain[None],
        narrowing_matrix,
        rotary_down.T,
        summary_scaling[None],
        table,
    )
    held = exchange(sent, sp, tp, True)

    query = query + moved
    turn = query[:, 128 : 128 + QK_ROPE]
    query = query[:, :128]
    own, partner = (
        jnp.einsum("hd,chd->hc", query, weight, preferred_element_type=F32).astype(BF16)
        for weight in (lookup_widening, lookup_other)
    )
    first, second = jnp.where(at[1] == 0, own, partner), jnp.where(at[1] == 0, partner, own)
    share = jnp.concatenate([first, second] * 4, axis=1)
    lane = lax.broadcasted_iota(jnp.int32, (2 * tp, 512), 1) // 128
    placed = jnp.where(lane == at[0], share, jnp.zeros((), BF16))
    moved = lax.ppermute(placed, "x", near)
    placed = placed + moved
    other = lax.ppermute(placed, "x", far)
    each = payload_widening.shape[0]
    parts = call(
        pack_payload_kernel,
        [shape((2, each, 256), BF16)] * 4,
        1_000_000,
        1_000_000,
        in_specs=[small, whole, whole],
        scratch_shapes=[pltpu.VMEM((each * 2 * tp, 128), F32)] * 2,
    )(at, payload_widening, payload_other)
    pieces = [parts[0]]
    for d in (1, 2, 3):
        pieces.append(lax.ppermute(parts[d], "x", [(i, (i + d) % 4) for i in range(4)]))
    turned = rotate(turn.astype(F32), F32(seqs * 0 + sp * tp * pos_local)).astype(BF16)
    turned = jnp.concatenate([turned, jnp.zeros_like(turned)], axis=1)

    piece = call(attend_kernel, shape((tp, 80, 512), BF16), 600_000_000, 1_300_000)(
        held, placed, other, turned
    )
    arrived = exchange(piece, sp, tp, False)
    weight = call(
        order_payload_kernel,
        shape((tp, each, 256), BF16),
        1_000_000,
        500_000,
        in_specs=[small] + [whole] * 4,
    )(at, *pieces)

    total = sp * tp * pos_local
    stored, rotary, first = call(
        finish_kernel,
        (shape((64, total), BF16), shape((8, total), BF16), shape((2, 128), BF16)),
        10_000_000,
        1_800_000,
    )(arrived, weight)
    return stored.T[None], rotary.T[None], first[None]


def solution(mesh):
    torus = Mesh(mesh.devices.reshape(mesh.shape["sp"], 4, 2), SP_TP)
    in_specs = (
        P(None, SP_TP, None),
        P(),
        P(),
        P(),
        P(),
        P(TP, None, None),
        P(TP, None, None),
        P("sp", TP, None),
        P("sp", TP, None),
    )
    out_specs = (P("sp", None, TP), P("sp", None, TP), P("sp", TP, None))

    return jax.shard_map(
        shards, mesh=torus, in_specs=in_specs, out_specs=out_specs, check_vma=False
    )
```

profile of v0, /device:TPU:1, one launch (start us, length us, event | category | flops | bytes accessed | tf_op | source)
XLA Modules:
  0.0 60.1 jit_solution(13490242844383209547)
XLA Ops:
  0.7 0.7 %maximum_maximum_fusion.mine_ref = bf16[2,256]{1,0:T(2,128)(2,1)S(1)} fusion(bf16[2,64]{1,0:T(2,128)(2,1)} %bitcast.31, bf16[2,128]{1,0:T(2,128)(2,1)} %bitcast.32, bf16[256]{0:T(256)(128)(2,1)S(1)} %pad.5.clone), kind=kLoop, calls=%fused_computation.30 | loop fusion | flops 3072 | bytes 2304 | tf_op jit(solution)/shard_map/concatenate | solution.py:198
  1.4 1.4 %collective-permute-start = (bf16[2,256]{1,0:T(2,128)(2,1)S(1)}, bf16[2,256]{1,0:T(2,128)(2,1)S(1)}, u32[]{:S(2)}, u32[]{:S(2)}) collective-permute-start(bf16[2,256]{1,0:T(2,128)(2,1)S(1)} %maximum_maximum_fusion.mine_ref), channel_id=1, source_target_pairs={{0,1},{1,0},{2,3},{3,2},{4,5},{5,4},{6,7},{7,6},{8,9},{9,8},{10,11... | collective-permute-start | bytes 3080 | tf_op jit(solution)/shard_map/ppermute | solution.py:201
  2.9 0.1 multiply_cosine_fusion
  3.1 1.6 %copy-done = bf16[16,32,2048]{2,1,0:T(8,128)(2,1)S(1)} copy-done((bf16[16,32,2048]{2,1,0:T(8,128)(2,1)S(1)}, bf16[16,32,2048]{2,1,0:T(8,128)(2,1)}, u32[]{:S(2)}) %copy-start) | copy-done | bytes 2097176
  4.7 1.6 %copy-done.1 = bf16[2048,512]{1,0:T(8,128)(2,1)S(1)} copy-done((bf16[2048,512]{1,0:T(8,128)(2,1)S(1)}, bf16[2048,512]{1,0:T(8,128)(2,1)}, u32[]{:S(2)}) %copy-start.1) | copy-done | bytes 2097176
  6.3 0.9 %copy-done.2 = bf16[2048,64]{0,1:T(8,128)(2,1)S(1)} copy-done((bf16[2048,64]{0,1:T(8,128)(2,1)S(1)}, bf16[2048,64]{0,1:T(8,128)(2,1)}, u32[]{:S(2)}) %copy-start.2) | copy-done | bytes 262168
  7.3 0.7 %copy-done.4 = f32[2048]{0:T(1024)S(1)} copy-done((f32[2048]{0:T(1024)S(1)}, f32[2048]{0:T(1024)}, u32[]{:S(2)}) %copy-start.4) | copy-done | bytes 8216
  8.0 0.7 %copy-done.5 = f32[512]{0:T(512)S(1)} copy-done((f32[512]{0:T(512)S(1)}, f32[512]{0:T(512)}, u32[]{:S(2)}) %copy-start.5) | copy-done | bytes 2072
  8.6 3.1 %shard_map.112 = bf16[16,32,640]{2,1,0:T(8,128)(2,1)} custom-call(bf16[512,2048]{1,0:T(8,128)(2,1)S(1)} %bitcast.25, f32[1,2048]{1,0:T(1,128)S(1)} %bitcast.27, bf16[2048,512]{1,0:T(8,128)(2,1)S(1)} %copy-done.1, bf16[64,2048]{1,0:T(8,128)(2,1)S(1)} %bitcast.26, f32[1,512]{1,0:T(1,128)S(1)} %bitcast.28, f32[2,32,64]{2,1,0:T(8,128)S(1)} %pad_maximum_fusion.cs_ref), custom_call_target="tpu_custom_call" | custom-call | flops 1300000000 | bytes 5000000 | tf_op jit(solution)/shard_map/pallas_call | solution.py:220
  11.8 9.8 %all-to-all-start = ((bf16[16,32,640]{2,1,0:T(8,128)(2,1)}), bf16[16,32,640]{2,1,0:T(8,128)(2,1)S(1)}, u32[]{:S(2)}, u32[]{:S(2)}) async-start(bf16[16,32,640]{2,1,0:T(8,128)(2,1)} %shard_map.112), calls=%async_computation | async-start | bytes 1310720 | tf_op jit(solution)/shard_map/all_to_all | solution.py:161
  21.7 0.6 shard_map.113
  22.2 1.3 %collective-permute-start.1 = (bf16[16,256]{1,0:T(8,128)(2,1)S(1)}, bf16[16,256]{1,0:T(8,128)(2,1)S(1)}, u32[]{:S(2)}, u32[]{:S(2)}) collective-permute-start(bf16[16,256]{1,0:T(8,128)(2,1)S(1)} %shard_map.113), channel_id=1, source_target_pairs={{0,2},{2,0},{4,6},{6,4},{1,3},{3,1},{5,7},{7,5},{8,10},{10,8},{12,... | collective-permute-start | bytes 24584 | tf_op jit(solution)/shard_map/ppermute | solution.py:210
  23.6 1.5 %collective-permute-done.1 = bf16[16,256]{1,0:T(8,128)(2,1)S(1)} collective-permute-done((bf16[16,256]{1,0:T(8,128)(2,1)S(1)}, bf16[16,256]{1,0:T(8,128)(2,1)S(1)}, u32[]{:S(2)}, u32[]{:S(2)}) %collective-permute-start.1) | collective-permute-done | bytes 8224 | tf_op jit(solution)/shard_map/ppermute | solution.py:210
  25.1 2.5 %collective-permute-start.2 = (bf16[16,256]{1,0:T(8,128)(2,1)S(1)}, bf16[16,256]{1,0:T(8,128)(2,1)S(1)}, u32[]{:S(2)}, u32[]{:S(2)}) collective-permute-start(bf16[16,256]{1,0:T(8,128)(2,1)S(1)} %add.36), channel_id=1, source_target_pairs={{0,6},{6,0},{2,4},{4,2},{1,7},{7,1},{3,5},{5,3},{8,14},{14,8},{10,... | collective-permute-start | bytes 24584 | tf_op jit(solution)/shard_map/ppermute | solution.py:212
  27.6 1.5 %collective-permute-done.2 = bf16[16,256]{1,0:T(8,128)(2,1)S(1)} collective-permute-done((bf16[16,256]{1,0:T(8,128)(2,1)S(1)}, bf16[16,256]{1,0:T(8,128)(2,1)S(1)}, u32[]{:S(2)}, u32[]{:S(2)}) %collective-permute-start.2) | collective-permute-done | bytes 8224 | tf_op jit(solution)/shard_map/ppermute | solution.py:212
  29.1 0.2 fusion.2
  29.4 0.3 fusion
  29.9 2.5 %collective-permute-done.4 = bf16[16,512]{1,0:T(8,128)(2,1)S(1)} collective-permute-done((bf16[16,512]{1,0:T(8,128)(2,1)S(1)}, bf16[16,512]{1,0:T(8,128)(2,1)S(1)}, u32[]{:S(2)}, u32[]{:S(2)}) %collective-permute-start.4) | collective-permute-done | bytes 16416 | tf_op jit(solution)/shard_map/ppermute | solution.py:246
  32.4 2.6 %collective-permute-start.5 = (bf16[16,512]{1,0:T(8,128)(2,1)S(1)}, bf16[16,512]{1,0:T(8,128)(2,1)S(1)}, u32[]{:S(2)}, u32[]{:S(2)}) collective-permute-start(bf16[16,512]{1,0:T(8,128)(2,1)S(1)} %fusion.14.a0_ref), channel_id=1, source_target_pairs={{0,6},{6,0},{2,4},{4,2},{1,7},{7,1},{3,5},{5,3},{8,14},{14,8},{10,... | collective-permute-start | bytes 49160 | tf_op jit(solution)/shard_map/ppermute | solution.py:248
  35.1 1.2 %collective-permute-done.5.a1_ref = bf16[16,512]{1,0:T(8,128)(2,1)S(1)} collective-permute-done((bf16[16,512]{1,0:T(8,128)(2,1)S(1)}, bf16[16,512]{1,0:T(8,128)(2,1)S(1)}, u32[]{:S(2)}, u32[]{:S(2)}) %collective-permute-start.5) | collective-permute-done | bytes 16416 | tf_op jit(solution)/shard_map/ppermute | solution.py:248
  36.3 1.4 %shard_map.114 = bf16[8,80,512]{2,1,0:T(8,128)(2,1)} custom-call(bf16[16,32,640]{2,1,0:T(8,128)(2,1)S(1)} %all-to-all-done.z_ref, bf16[16,512]{1,0:T(8,128)(2,1)S(1)} %fusion.14.a0_ref, bf16[16,512]{1,0:T(8,128)(2,1)S(1)} %collective-permute-done.5.a1_ref, bf16[16,128]{1,0:T(8,128)(2,1)S(1)} %fusion.10.t_ref), custom_call_target="tpu_custom_call" | custom-call | flops 600000000 | bytes 1300000 | tf_op jit(solution)/shard_map/pallas_call | solution.py:264
  37.7 8.6 %all-to-all-start.1 = ((bf16[8,80,512]{2,1,0:T(8,128)(2,1)}), bf16[8,80,512]{2,1,0:T(8,128)(2,1)S(1)}, u32[]{:S(2)}, u32[]{:S(2)}) async-start(bf16[8,80,512]{2,1,0:T(8,128)(2,1)} %shard_map.114), calls=%async_computation.1 | async-start | bytes 1310720 | tf_op jit(solution)/shard_map/all_to_all | solution.py:161
  46.3 0.4 collective-permute-start.6
  46.7 1.3 %collective-permute-done.6.other_ref = bf16[64,16,128]{2,1,0:T(8,128)(2,1)S(1)} collective-permute-done((bf16[64,16,128]{2,1,0:T(8,128)(2,1)S(1)}, bf16[64,16,128]{2,1,0:T(8,128)(2,1)S(1)}, u32[]{:S(2)}, u32[]{:S(2)}) %collective-permute-start.6) | collective-permute-done | bytes 262176 | tf_op jit(solution)/shard_map/ppermute | solution.py:197
  48.0 0.8 %shard_map.115 = (bf16[2,64,256]{2,1,0:T(8,128)(2,1)S(1)}, bf16[2,64,256]{2,1,0:T(8,128)(2,1)S(1)}, bf16[2,64,256]{2,1,0:T(8,128)(2,1)S(1)}, bf16[2,64,256]{2,1,0:T(8,128)(2,1)S(1)}) custom-call(s32[2]{0:T(128)S(1)} %pad_add_fusion.at_ref, bf16[64,16,128]{2,1,0:T(8,128)(2,1)S(1)} %copy-done.3, bf16[64,16,128]{2,1,0:T(8,128)(2,1)S(1)} %collective-permute-done.6.other_ref), custom_call_target="tpu_custom_call" | custom-call | flops 1000000 | bytes 1000000 | tf_op jit(solution)/shard_map/pallas_call | solution.py:250
  48.8 0.6 %collective-permute-start.7 = (bf16[2,64,256]{2,1,0:T(8,128)(2,1)S(1)}, bf16[2,64,256]{2,1,0:T(8,128)(2,1)S(1)}, u32[]{:S(2)}, u32[]{:S(2)}) collective-permute-start(bf16[2,64,256]{2,1,0:T(8,128)(2,1)S(1)} %get-tuple-element.11), channel_id=1, source_target_pairs={{0,2},{2,4},{4,6},{6,0},{1,3},{3,5},{5,7},{7,1},{8,10},{10,12},{12... | collective-permute-start | bytes 196616 | tf_op jit(solution)/shard_map/ppermute | solution.py:260
  49.4 2.3 %collective-permute-start.8 = (bf16[2,64,256]{2,1,0:T(8,128)(2,1)S(1)}, bf16[2,64,256]{2,1,0:T(8,128)(2,1)S(1)}, u32[]{:S(2)}, u32[]{:S(2)}) collective-permute-start(bf16[2,64,256]{2,1,0:T(8,128)(2,1)S(1)} %get-tuple-element.12), channel_id=1, source_target_pairs={{0,4},{2,6},{4,0},{6,2},{1,5},{3,7},{5,1},{7,3},{8,12},{10,14},{12... | collective-permute-start | bytes 196616 | tf_op jit(solution)/shard_map/ppermute | solution.py:260
  51.7 0.4 collective-permute-start.9
  52.1 3.7 %collective-permute-done.7.p1_ref = bf16[2,64,256]{2,1,0:T(8,128)(2,1)S(1)} collective-permute-done((bf16[2,64,256]{2,1,0:T(8,128)(2,1)S(1)}, bf16[2,64,256]{2,1,0:T(8,128)(2,1)S(1)}, u32[]{:S(2)}, u32[]{:S(2)}) %collective-permute-start.7) | collective-permute-done | bytes 65568 | tf_op jit(solution)/shard_map/ppermute | solution.py:260
  55.8 2.4 %collective-permute-done.8.p2_ref = bf16[2,64,256]{2,1,0:T(8,128)(2,1)S(1)} collective-permute-done((bf16[2,64,256]{2,1,0:T(8,128)(2,1)S(1)}, bf16[2,64,256]{2,1,0:T(8,128)(2,1)S(1)}, u32[]{:S(2)}, u32[]{:S(2)}) %collective-permute-start.8) | collective-permute-done | bytes 65568 | tf_op jit(solution)/shard_map/ppermute | solution.py:260
  58.2 0.6 shard_map.116.w_ref
  58.7 1.4 %shard_map.117 = (bf16[64,4096]{1,0:T(8,128)(2,1)}, bf16[8,4096]{1,0:T(8,128)(2,1)}, bf16[2,128]{1,0:T(2,128)(2,1)}) custom-call(bf16[8,80,512]{2,1,0:T(8,128)(2,1)S(1)} %all-to-all-done.1.y_ref, bf16[8,64,256]{2,1,0:T(8,128)(2,1)S(1)} %shard_map.116.w_ref), custom_call_target="tpu_custom_call" | custom-call | flops 10000000 | bytes 1800000 | tf_op jit(solution)/shard_map/pallas_call | solution.py:277
  (36 shorter events, 0.8 us)
Async XLA Ops:
  1.4 20.3 %collective-permute-start = (bf16[2,256]{1,0:T(2,128)(2,1)S(1)}, bf16[2,256]{1,0:T(2,128)(2,1)S(1)}, u32[]{:S(2)}, u32[]{:S(2)}) collective-permute-start(bf16[2,256]{1,0:T(2,128)(2,1)S(1)} %maximum_maximum_fusion.mine_ref), channel_id=1, source_target_pairs={{0,1},{1,0},{2,3},{3,2},{4,5},{5,4},{6,7},{7,6},{8,9},{9,8},{10,11... | collective-permute-start | bytes 3080 | tf_op jit(solution)/shard_map/ppermute | solution.py:201
  2.8 26.6 %collective-permute-start.3 = (bf16[64,16,128]{2,1,0:T(8,128)(2,1)}, bf16[64,16,128]{2,1,0:T(8,128)(2,1)S(1)}, u32[]{:S(2)}, u32[]{:S(2)}) collective-permute-start(bf16[64,16,128]{2,1,0:T(8,128)(2,1)} %param.14), channel_id=1, source_target_pairs={{0,1},{1,0},{2,3},{3,2},{4,5},{5,4},{6,7},{7,6},{8,9},{9,8},{10,11... | collective-permute-start | bytes 786440 | tf_op jit(solution)/shard_map/ppermute | solution.py:196
  3.1 1.6 %copy-start = (bf16[16,32,2048]{2,1,0:T(8,128)(2,1)S(1)}, bf16[16,32,2048]{2,1,0:T(8,128)(2,1)}, u32[]{:S(2)}) copy-start(bf16[16,32,2048]{2,1,0:T(8,128)(2,1)} %param.9) | copy-start | bytes 6291460
  4.7 1.6 %copy-start.1 = (bf16[2048,512]{1,0:T(8,128)(2,1)S(1)}, bf16[2048,512]{1,0:T(8,128)(2,1)}, u32[]{:S(2)}) copy-start(bf16[2048,512]{1,0:T(8,128)(2,1)} %w_ref.1) | copy-start | bytes 6291460
  6.3 0.9 %copy-start.2 = (bf16[2048,64]{0,1:T(8,128)(2,1)S(1)}, bf16[2048,64]{0,1:T(8,128)(2,1)}, u32[]{:S(2)}) copy-start(bf16[2048,64]{0,1:T(8,128)(2,1)} %param.12) | copy-start | bytes 786436
  7.3 0.7 %copy-start.4 = (f32[2048]{0:T(1024)S(1)}, f32[2048]{0:T(1024)}, u32[]{:S(2)}) copy-start(f32[2048]{0:T(1024)} %param.10) | copy-start | bytes 24580
  8.0 0.7 %copy-start.5 = (f32[512]{0:T(512)S(1)}, f32[512]{0:T(512)}, u32[]{:S(2)}) copy-start(f32[512]{0:T(512)} %param.13) | copy-start | bytes 6148
  11.8 24.6 %all-to-all-start = ((bf16[16,32,640]{2,1,0:T(8,128)(2,1)}), bf16[16,32,640]{2,1,0:T(8,128)(2,1)S(1)}, u32[]{:S(2)}, u32[]{:S(2)}) async-start(bf16[16,32,640]{2,1,0:T(8,128)(2,1)} %shard_map.112), calls=%async_computation | async-start | bytes 1310720 | tf_op jit(solution)/shard_map/all_to_all | solution.py:161
  21.7 7.5 %copy-start.6 = (bf16[64,16,128]{2,1,0:T(8,128)(2,1)S(1)}, bf16[64,16,128]{2,1,0:T(8,128)(2,1)}, u32[]{:S(2)}) copy-start(bf16[64,16,128]{2,1,0:T(8,128)(2,1)} %param.14) | copy-start | bytes 786436
  22.2 2.9 %collective-permute-start.1 = (bf16[16,256]{1,0:T(8,128)(2,1)S(1)}, bf16[16,256]{1,0:T(8,128)(2,1)S(1)}, u32[]{:S(2)}, u32[]{:S(2)}) collective-permute-start(bf16[16,256]{1,0:T(8,128)(2,1)S(1)} %shard_map.113), channel_id=1, source_target_pairs={{0,2},{2,0},{4,6},{6,4},{1,3},{3,1},{5,7},{7,5},{8,10},{10,8},{12,... | collective-permute-start | bytes 24584 | tf_op jit(solution)/shard_map/ppermute | solution.py:210
  25.1 4.0 %collective-permute-start.2 = (bf16[16,256]{1,0:T(8,128)(2,1)S(1)}, bf16[16,256]{1,0:T(8,128)(2,1)S(1)}, u32[]{:S(2)}, u32[]{:S(2)}) collective-permute-start(bf16[16,256]{1,0:T(8,128)(2,1)S(1)} %add.36), channel_id=1, source_target_pairs={{0,6},{6,0},{2,4},{4,2},{1,7},{7,1},{3,5},{5,3},{8,14},{14,8},{10,... | collective-permute-start | bytes 24584 | tf_op jit(solution)/shard_map/ppermute | solution.py:212
  29.4 16.9 %copy-start.3 = (bf16[64,16,128]{2,1,0:T(8,128)(2,1)S(1)}, bf16[64,16,128]{2,1,0:T(8,128)(2,1)}, u32[]{:S(2)}) copy-start(bf16[64,16,128]{2,1,0:T(8,128)(2,1)} %own_ref.1) | copy-start | bytes 786436
  29.8 2.7 %collective-permute-start.4 = (bf16[16,512]{1,0:T(8,128)(2,1)S(1)}, bf16[16,512]{1,0:T(8,128)(2,1)S(1)}, u32[]{:S(2)}, u32[]{:S(2)}) collective-permute-start(bf16[16,512]{1,0:T(8,128)(2,1)S(1)} %fusion.4), channel_id=1, source_target_pairs={{0,2},{2,0},{4,6},{6,4},{1,3},{3,1},{5,7},{7,5},{8,10},{10,8},{12,... | collective-permute-start | bytes 49160 | tf_op jit(solution)/shard_map/ppermute | solution.py:246
  32.4 3.9 %collective-permute-start.5 = (bf16[16,512]{1,0:T(8,128)(2,1)S(1)}, bf16[16,512]{1,0:T(8,128)(2,1)S(1)}, u32[]{:S(2)}, u32[]{:S(2)}) collective-permute-start(bf16[16,512]{1,0:T(8,128)(2,1)S(1)} %fusion.14.a0_ref), channel_id=1, source_target_pairs={{0,6},{6,0},{2,4},{4,2},{1,7},{7,1},{3,5},{5,3},{8,14},{14,8},{10,... | collective-permute-start | bytes 49160 | tf_op jit(solution)/shard_map/ppermute | solution.py:248
  37.7 21.0 %all-to-all-start.1 = ((bf16[8,80,512]{2,1,0:T(8,128)(2,1)}), bf16[8,80,512]{2,1,0:T(8,128)(2,1)S(1)}, u32[]{:S(2)}, u32[]{:S(2)}) async-start(bf16[8,80,512]{2,1,0:T(8,128)(2,1)} %shard_map.114), calls=%async_computation.1 | async-start | bytes 1310720 | tf_op jit(solution)/shard_map/all_to_all | solution.py:161
  46.3 1.7 %collective-permute-start.6 = (bf16[64,16,128]{2,1,0:T(8,128)(2,1)S(1)}, bf16[64,16,128]{2,1,0:T(8,128)(2,1)S(1)}, u32[]{:S(2)}, u32[]{:S(2)}) collective-permute-start(bf16[64,16,128]{2,1,0:T(8,128)(2,1)S(1)} %copy-done.3), channel_id=1, source_target_pairs={{0,1},{1,0},{2,3},{3,2},{4,5},{5,4},{6,7},{7,6},{8,9},{9,8},{10,11... | collective-permute-start | bytes 786440 | tf_op jit(solution)/shard_map/ppermute | solution.py:197
  48.8 7.0 %collective-permute-start.7 = (bf16[2,64,256]{2,1,0:T(8,128)(2,1)S(1)}, bf16[2,64,256]{2,1,0:T(8,128)(2,1)S(1)}, u32[]{:S(2)}, u32[]{:S(2)}) collective-permute-start(bf16[2,64,256]{2,1,0:T(8,128)(2,1)S(1)} %get-tuple-element.11), channel_id=1, source_target_pairs={{0,2},{2,4},{4,6},{6,0},{1,3},{3,5},{5,7},{7,1},{8,10},{10,12},{12... | collective-permute-start | bytes 196616 | tf_op jit(solution)/shard_map/ppermute | solution.py:260
  49.4 8.7 %collective-permute-start.8 = (bf16[2,64,256]{2,1,0:T(8,128)(2,1)S(1)}, bf16[2,64,256]{2,1,0:T(8,128)(2,1)S(1)}, u32[]{:S(2)}, u32[]{:S(2)}) collective-permute-start(bf16[2,64,256]{2,1,0:T(8,128)(2,1)S(1)} %get-tuple-element.12), channel_id=1, source_target_pairs={{0,4},{2,6},{4,0},{6,2},{1,5},{3,7},{5,1},{7,3},{8,12},{10,14},{12... | collective-permute-start | bytes 196616 | tf_op jit(solution)/shard_map/ppermute | solution.py:260
  51.7 6.4 %collective-permute-start.9 = (bf16[2,64,256]{2,1,0:T(8,128)(2,1)S(1)}, bf16[2,64,256]{2,1,0:T(8,128)(2,1)S(1)}, u32[]{:S(2)}, u32[]{:S(2)}) collective-permute-start(bf16[2,64,256]{2,1,0:T(8,128)(2,1)S(1)} %get-tuple-element.13), channel_id=1, source_target_pairs={{0,6},{2,0},{4,2},{6,4},{1,7},{3,1},{5,3},{7,5},{8,14},{10,8},{12,... | collective-permute-start | bytes 196616 | tf_op jit(solution)/shard_map/ppermute | solution.py:260
where the time goes:
time: 60.6 us; the launch traced here: 60.1 us
  starting transfers between devices  29.9 us (49%)
  waiting for transfers between devices  14.2 us (23%)
  Pallas kernels  7.82 us (13%)
  local copies, waits for them, and re-layouts  5.7 us (9%)
  other arithmetic  1.27 us (2%)
  between operations  0.74 us (1%)
    all_to_all x2, starting transfers between devices, exchange(): lax.all_to_all(array, SP_TP, 0, 0, tiled=True, axis_index_groups=groups)  18.3 us
    ppermute x3, waiting for transfers between devices, shards(): lax.ppermute(parts[d], 'x', [(i, (i + d) % 4) for i in range(4)])  6.04 us
    unnamed x14, local copies, waits for them, and re-layouts  5.51 us
    ppermute x3, starting transfers between devices, shards(): lax.ppermute(parts[d], 'x', [(i, (i + d) % 4) for i in range(4)])  3.32 us
    pallas_call x1, Pallas kernels, shards(): call(project_kernel, shape((seqs, pos_local, 640), BF16), 1300000000, 500...  3.13 us
    ppermute x1, starting transfers between devices, shards(): other = lax.ppermute(placed, 'x', far)  2.56 us
    ppermute x1, waiting for transfers between devices, shards(): moved = lax.ppermute(placed, 'x', near)  2.5 us
    ppermute x1, starting transfers between devices, shards(): moved = lax.ppermute(query, 'x', far)  2.48 us
  transfers between devices with their start and end apart: 12, of which 7 were waited for; matrix products, arithmetic and copies ran while one was open for 2% of the time, Pallas kernels for 8%

commit v1 on v0

--- a/solution.py
+++ b/solution.py
@@ -61,35 +61,37 @@
 
 
 def project_kernel(x_ref, gain_ref, w_ref, r_ref, scal_ref, cs_ref, out_ref):
-    rows = x_ref.shape[0]
-    step = 128
-    gain = gain_ref[...]
-    scal = scal_ref[...]
-    seqs = step // 32
-    cos = jnp.concatenate([cs_ref[0]] * seqs, axis=0)
-    sin = jnp.concatenate([cs_ref[1]] * seqs, axis=0)
-    for i in range(rows // step):
-        x = x_ref[i * step : (i + 1) * step, :].astype(F32)
-        mean = jnp.mean(x * x, axis=-1, keepdims=True)
-        normed = (x * lax.rsqrt(mean + norm_eps) * gain).astype(BF16)
-        lat = jnp.dot(normed, w_ref[...], preferred_element_type=F32).astype(BF16).astype(F32)
-        rot = lax.dot_general(normed, r_ref[...], LAST, preferred_element_type=F32)
-        rot = rot.astype(BF16).astype(F32)
-        mean = jnp.mean(lat * lat, axis=-1, keepdims=True)
-        lat = (lat * lax.rsqrt(mean + norm_eps) * scal).astype(BF16)
-        swapped = jnp.concatenate([rot[:, 32:], rot[:, :32]], axis=1)
-        rot = rot * cos + swapped * sin
-        rot = jnp.concatenate([rot, jnp.zeros_like(rot)], axis=1).astype(BF16)
-        for s in range(seqs):
-            slot = out_ref.shape[0] - 1 - (i * seqs + s)
-            out_ref[slot, :, 0:512] = lat[s * 32 : (s + 1) * 32]
-            out_ref[slot, :, 512:640] = rot[s * 32 : (s + 1) * 32]
+    count = out_ref.shape[0]
+    x = x_ref[...].astype(F32)
+    scale = lax.rsqrt(jnp.mean(x * x, axis=-1, keepdims=True) + norm_eps)
+    gained = (x * gain_ref[...]).astype(BF16)
+    lat = jnp.dot(gained, w_ref[...], preferred_element_type=F32)
+    rot = lax.dot_general(gained, r_ref[...], LAST, preferred_element_type=F32)
+    lat = (lat * scale).astype(BF16).astype(F32)
+    rot = (rot * scale).astype(BF16).astype(F32)
+    mean = jnp.mean(lat * lat, axis=-1, keepdims=True)
+    lat = (lat * lax.rsqrt(mean + norm_eps) * scal_ref[...]).astype(BF16)
+    cos = jnp.concatenate([cs_ref[0]] * count, axis=0)
+    sin = jnp.concatenate([cs_ref[1]] * count, axis=0)
+    swapped = jnp.concatenate([rot[:, 32:], rot[:, :32]], axis=1)
+    rot = rot * cos + swapped * sin
+    for s in range(count):
+        slot = count - 1 - s
+        at = s * 32
+        pair = jnp.concatenate([rot[at : at + 16], rot[at + 16 : at + 32]], axis=1)
+        out_ref[slot, :, 0:512] = lat[at : at + 16]
+        out_ref[slot, :, 512:1024] = lat[at + 16 : at + 32]
+        out_ref[slot, :, 1024:1152] = pair.astype(BF16)
 
 
 def attend_kernel(z_ref, a0_ref, a1_ref, t_ref, out_ref):
-    order = range(z_ref.shape[0] - 1, -1, -1)
-    lat = jnp.concatenate([z_ref[i, :, 0:512] for i in order], axis=0)
-    rot = jnp.concatenate([z_ref[i, :, 512:640] for i in order], axis=0)
+    lats, rots = [], []
+    for i in range(z_ref.shape[0] - 1, -1, -1):
+        lats += [z_ref[i, :, 0:512], z_ref[i, :, 512:1024]]
+        pair = z_ref[i, :, 1024:1152]
+        rots += [pair, jnp.concatenate([pair[:, 64:], pair[:, :64]], axis=1)]
+    lat = jnp.concatenate(lats, axis=0)
+    rot = jnp.concatenate(rots, axis=0)
     absorbed = a0_ref[...] + a1_ref[...]
     scores = lax.dot_general(absorbed, lat, LAST, preferred_element_type=F32)
     scores = scores + lax.dot_general(t_ref[...], rot, LAST, preferred_element_type=F32)
@@ -207,9 +209,9 @@
         in_specs=[small, whole, whole],
     )(at, mine, partner)
     near, far = [(0, 1), (1, 0), (2, 3), (3, 2)], [(0, 3), (3, 0), (1, 2), (2, 1)]
+    moved = lax.ppermute(query, "x", far)
+    query = query + moved
     moved = lax.ppermute(query, "x", near)
-    query = query + moved
-    moved = lax.ppermute(query, "x", far)
 
     positions = (block * pos_local + jnp.arange(pos_local, dtype=jnp.int32)).astype(F32)
     angles = positions[:, None] * frequencies()[None, :]
@@ -219,7 +221,7 @@
     )
     sent = call(
         project_kernel,
-        shape((seqs, pos_local, 640), BF16),
+        shape((seqs, pos_local // 2, 1152), BF16),
         1_300_000_000,
         5_000_000,
     )(

time: 60.6 us -> 60.6 us (level)
  waiting for transfers between devices: 14.2 us -> 15.4 us
  starting transfers between devices: 29.9 us -> 28.7 us
    ppermute x1, starting transfers between devices: 1.29 us -> 0.01 us  [shards(): moved = lax.ppermute(query, 'x', near)]
    ppermute x1, waiting for transfers between devices: 1.53 us -> 2.78 us  [shards(): moved = lax.ppermute(query, 'x', near)]
where the time goes in v1:
time: 60.6 us; the launch traced here: 60.1 us
  starting transfers between devices  28.7 us (47%)
  waiting for transfers between devices  15.4 us (25%)
  Pallas kernels  7.8 us (13%)
  local copies, waits for them, and re-layouts  5.7 us (9%)
  other arithmetic  1.27 us (2%)
  between operations  0.74 us (1%)
    all_to_all x2, starting transfers between devices, exchange(): lax.all_to_all(array, SP_TP, 0, 0, tiled=True, axis_index_groups=groups)  18.3 us
    ppermute x3, waiting for transfers between devices, shards(): lax.ppermute(parts[d], 'x', [(i, (i + d) % 4) for i in range(4)])  6.04 us
    unnamed x14, local copies, waits for them, and re-layouts  5.51 us
    ppermute x3, starting transfers between devices, shards(): lax.ppermute(parts[d], 'x', [(i, (i + d) % 4) for i in range(4)])  3.32 us
    pallas_call x1, Pallas kernels, shards(): call(project_kernel, shape((seqs, pos_local // 2, 1152), BF16), 130000000...  3.05 us
    ppermute x1, waiting for transfers between devices, shards(): moved = lax.ppermute(query, 'x', near)  2.78 us
    ppermute x1, starting transfers between devices, shards(): moved = lax.ppermute(query, 'x', far)  2.56 us
    ppermute x1, starting transfers between devices, shards(): other = lax.ppermute(placed, 'x', far)  2.56 us
  transfers between devices with their start and end apart: 12, of which 7 were waited for; matrix products, arithmetic and copies ran while one was open for 2% of the time, Pallas kernels for 8%

profile of v1, /device:TPU:1, one launch (start us, length us, event | category | flops | bytes accessed | tf_op | source)
XLA Modules:
  0.0 60.1 jit_solution(5427582891515114012)
XLA Ops:
  0.7 0.7 %maximum_maximum_fusion.mine_ref = bf16[2,256]{1,0:T(2,128)(2,1)S(1)} fusion(bf16[2,64]{1,0:T(2,128)(2,1)} %bitcast.31, bf16[2,128]{1,0:T(2,128)(2,1)} %bitcast.32, bf16[256]{0:T(256)(128)(2,1)S(1)} %pad.5.clone), kind=kLoop, calls=%fused_computation.30 | loop fusion | flops 3072 | bytes 2304 | tf_op jit(solution)/shard_map/concatenate | solution.py:200
  1.4 1.4 %collective-permute-start = (bf16[2,256]{1,0:T(2,128)(2,1)S(1)}, bf16[2,256]{1,0:T(2,128)(2,1)S(1)}, u32[]{:S(2)}, u32[]{:S(2)}) collective-permute-start(bf16[2,256]{1,0:T(2,128)(2,1)S(1)} %maximum_maximum_fusion.mine_ref), channel_id=1, source_target_pairs={{0,1},{1,0},{2,3},{3,2},{4,5},{5,4},{6,7},{7,6},{8,9},{9,8},{10,11... | collective-permute-start | bytes 3080 | tf_op jit(solution)/shard_map/ppermute | solution.py:203
  2.9 0.1 multiply_cosine_fusion
  3.1 1.6 %copy-done = bf16[16,32,2048]{2,1,0:T(8,128)(2,1)S(1)} copy-done((bf16[16,32,2048]{2,1,0:T(8,128)(2,1)S(1)}, bf16[16,32,2048]{2,1,0:T(8,128)(2,1)}, u32[]{:S(2)}) %copy-start) | copy-done | bytes 2097176
  4.7 1.6 %copy-done.1 = bf16[2048,512]{1,0:T(8,128)(2,1)S(1)} copy-done((bf16[2048,512]{1,0:T(8,128)(2,1)S(1)}, bf16[2048,512]{1,0:T(8,128)(2,1)}, u32[]{:S(2)}) %copy-start.1) | copy-done | bytes 2097176
  6.3 0.9 %copy-done.2 = bf16[2048,64]{0,1:T(8,128)(2,1)S(1)} copy-done((bf16[2048,64]{0,1:T(8,128)(2,1)S(1)}, bf16[2048,64]{0,1:T(8,128)(2,1)}, u32[]{:S(2)}) %copy-start.2) | copy-done | bytes 262168
  7.3 0.7 %copy-done.4 = f32[2048]{0:T(1024)S(1)} copy-done((f32[2048]{0:T(1024)S(1)}, f32[2048]{0:T(1024)}, u32[]{:S(2)}) %copy-start.4) | copy-done | bytes 8216
  8.0 0.7 %copy-done.5 = f32[512]{0:T(512)S(1)} copy-done((f32[512]{0:T(512)S(1)}, f32[512]{0:T(512)}, u32[]{:S(2)}) %copy-start.5) | copy-done | bytes 2072
  8.6 3.1 %shard_map.112 = bf16[16,16,1152]{2,1,0:T(8,128)(2,1)} custom-call(bf16[512,2048]{1,0:T(8,128)(2,1)S(1)} %bitcast.25, f32[1,2048]{1,0:T(1,128)S(1)} %bitcast.27, bf16[2048,512]{1,0:T(8,128)(2,1)S(1)} %copy-done.1, bf16[64,2048]{1,0:T(8,128)(2,1)S(1)} %bitcast.26, f32[1,512]{1,0:T(1,128)S(1)} %bitcast.28, f32[2,32,64]{2,1,0:T(8,128)S(1)} %pad_maximum_fusion.cs_ref), custom_call_target="tpu_custom_call" | custom-call | flops 1300000000 | bytes 5000000 | tf_op jit(solution)/shard_map/pallas_call | solution.py:222
  11.7 9.8 %all-to-all-start = ((bf16[16,16,1152]{2,1,0:T(8,128)(2,1)}), bf16[16,16,1152]{2,1,0:T(8,128)(2,1)S(1)}, u32[]{:S(2)}, u32[]{:S(2)}) async-start(bf16[16,16,1152]{2,1,0:T(8,128)(2,1)} %shard_map.112), calls=%async_computation | async-start | bytes 1179648 | tf_op jit(solution)/shard_map/all_to_all | solution.py:163
  21.6 0.6 shard_map.113
  22.1 2.6 %collective-permute-start.1 = (bf16[16,256]{1,0:T(8,128)(2,1)S(1)}, bf16[16,256]{1,0:T(8,128)(2,1)S(1)}, u32[]{:S(2)}, u32[]{:S(2)}) collective-permute-start(bf16[16,256]{1,0:T(8,128)(2,1)S(1)} %shard_map.113), channel_id=1, source_target_pairs={{0,6},{6,0},{2,4},{4,2},{1,7},{7,1},{3,5},{5,3},{8,14},{14,8},{10,... | collective-permute-start | bytes 24584 | tf_op jit(solution)/shard_map/ppermute | solution.py:212
  24.7 1.5 %collective-permute-done.1 = bf16[16,256]{1,0:T(8,128)(2,1)S(1)} collective-permute-done((bf16[16,256]{1,0:T(8,128)(2,1)S(1)}, bf16[16,256]{1,0:T(8,128)(2,1)S(1)}, u32[]{:S(2)}, u32[]{:S(2)}) %collective-permute-start.1) | collective-permute-done | bytes 8224 | tf_op jit(solution)/shard_map/ppermute | solution.py:212
  26.2 2.8 %collective-permute-done.2 = bf16[16,256]{1,0:T(8,128)(2,1)S(1)} collective-permute-done((bf16[16,256]{1,0:T(8,128)(2,1)S(1)}, bf16[16,256]{1,0:T(8,128)(2,1)S(1)}, u32[]{:S(2)}, u32[]{:S(2)}) %collective-permute-start.2) | collective-permute-done | bytes 8224 | tf_op jit(solution)/shard_map/ppermute | solution.py:214
  29.0 0.2 fusion.2
  29.3 0.3 fusion
  29.5 0.1 concatenate.22
  29.8 2.5 %collective-permute-done.4 = bf16[16,512]{1,0:T(8,128)(2,1)S(1)} collective-permute-done((bf16[16,512]{1,0:T(8,128)(2,1)S(1)}, bf16[16,512]{1,0:T(8,128)(2,1)S(1)}, u32[]{:S(2)}, u32[]{:S(2)}) %collective-permute-start.4) | collective-permute-done | bytes 16416 | tf_op jit(solution)/shard_map/ppermute | solution.py:248
  32.4 2.6 %collective-permute-start.5 = (bf16[16,512]{1,0:T(8,128)(2,1)S(1)}, bf16[16,512]{1,0:T(8,128)(2,1)S(1)}, u32[]{:S(2)}, u32[]{:S(2)}) collective-permute-start(bf16[16,512]{1,0:T(8,128)(2,1)S(1)} %fusion.14.a0_ref), channel_id=1, source_target_pairs={{0,6},{6,0},{2,4},{4,2},{1,7},{7,1},{3,5},{5,3},{8,14},{14,8},{10,... | collective-permute-start | bytes 49160 | tf_op jit(solution)/shard_map/ppermute | solution.py:250
  35.0 1.2 %collective-permute-done.5.a1_ref = bf16[16,512]{1,0:T(8,128)(2,1)S(1)} collective-permute-done((bf16[16,512]{1,0:T(8,128)(2,1)S(1)}, bf16[16,512]{1,0:T(8,128)(2,1)S(1)}, u32[]{:S(2)}, u32[]{:S(2)}) %collective-permute-start.5) | collective-permute-done | bytes 16416 | tf_op jit(solution)/shard_map/ppermute | solution.py:250
  36.2 1.5 %shard_map.114 = bf16[8,80,512]{2,1,0:T(8,128)(2,1)} custom-call(bf16[16,16,1152]{2,1,0:T(8,128)(2,1)S(1)} %all-to-all-done.z_ref, bf16[16,512]{1,0:T(8,128)(2,1)S(1)} %fusion.14.a0_ref, bf16[16,512]{1,0:T(8,128)(2,1)S(1)} %collective-permute-done.5.a1_ref, bf16[16,128]{1,0:T(8,128)(2,1)S(1)} %fusion.10.t_ref), custom_call_target="tpu_custom_call" | custom-call | flops 600000000 | bytes 1300000 | tf_op jit(solution)/shard_map/pallas_call | solution.py:266
  37.7 8.5 %all-to-all-start.1 = ((bf16[8,80,512]{2,1,0:T(8,128)(2,1)}), bf16[8,80,512]{2,1,0:T(8,128)(2,1)S(1)}, u32[]{:S(2)}, u32[]{:S(2)}) async-start(bf16[8,80,512]{2,1,0:T(8,128)(2,1)} %shard_map.114), calls=%async_computation.1 | async-start | bytes 1310720 | tf_op jit(solution)/shard_map/all_to_all | solution.py:163
  46.2 0.4 collective-permute-start.6
  46.6 1.3 %collective-permute-done.6.other_ref = bf16[64,16,128]{2,1,0:T(8,128)(2,1)S(1)} collective-permute-done((bf16[64,16,128]{2,1,0:T(8,128)(2,1)S(1)}, bf16[64,16,128]{2,1,0:T(8,128)(2,1)S(1)}, u32[]{:S(2)}, u32[]{:S(2)}) %collective-permute-start.6) | collective-permute-done | bytes 262176 | tf_op jit(solution)/shard_map/ppermute | solution.py:199
  48.0 0.8 %shard_map.115 = (bf16[2,64,256]{2,1,0:T(8,128)(2,1)S(1)}, bf16[2,64,256]{2,1,0:T(8,128)(2,1)S(1)}, bf16[2,64,256]{2,1,0:T(8,128)(2,1)S(1)}, bf16[2,64,256]{2,1,0:T(8,128)(2,1)S(1)}) custom-call(s32[2]{0:T(128)S(1)} %pad_add_fusion.at_ref, bf16[64,16,128]{2,1,0:T(8,128)(2,1)S(1)} %copy-done.3, bf16[64,16,128]{2,1,0:T(8,128)(2,1)S(1)} %collective-permute-done.6.other_ref), custom_call_target="tpu_custom_call" | custom-call | flops 1000000 | bytes 1000000 | tf_op jit(solution)/shard_map/pallas_call | solution.py:252
  48.8 0.6 %collective-permute-start.7 = (bf16[2,64,256]{2,1,0:T(8,128)(2,1)S(1)}, bf16[2,64,256]{2,1,0:T(8,128)(2,1)S(1)}, u32[]{:S(2)}, u32[]{:S(2)}) collective-permute-start(bf16[2,64,256]{2,1,0:T(8,128)(2,1)S(1)} %get-tuple-element.11), channel_id=1, source_target_pairs={{0,2},{2,4},{4,6},{6,0},{1,3},{3,5},{5,7},{7,1},{8,10},{10,12},{12... | collective-permute-start | bytes 196616 | tf_op jit(solution)/shard_map/ppermute | solution.py:262
  49.4 2.3 %collective-permute-start.8 = (bf16[2,64,256]{2,1,0:T(8,128)(2,1)S(1)}, bf16[2,64,256]{2,1,0:T(8,128)(2,1)S(1)}, u32[]{:S(2)}, u32[]{:S(2)}) collective-permute-start(bf16[2,64,256]{2,1,0:T(8,128)(2,1)S(1)} %get-tuple-element.12), channel_id=1, source_target_pairs={{0,4},{2,6},{4,0},{6,2},{1,5},{3,7},{5,1},{7,3},{8,12},{10,14},{12... | collective-permute-start | bytes 196616 | tf_op jit(solution)/shard_map/ppermute | solution.py:262
  51.7 0.4 collective-permute-start.9
  52.1 3.7 %collective-permute-done.7.p1_ref = bf16[2,64,256]{2,1,0:T(8,128)(2,1)S(1)} collective-permute-done((bf16[2,64,256]{2,1,0:T(8,128)(2,1)S(1)}, bf16[2,64,256]{2,1,0:T(8,128)(2,1)S(1)}, u32[]{:S(2)}, u32[]{:S(2)}) %collective-permute-start.7) | collective-permute-done | bytes 65568 | tf_op jit(solution)/shard_map/ppermute | solution.py:262
  55.8 2.4 %collective-permute-done.8.p2_ref = bf16[2,64,256]{2,1,0:T(8,128)(2,1)S(1)} collective-permute-done((bf16[2,64,256]{2,1,0:T(8,128)(2,1)S(1)}, bf16[2,64,256]{2,1,0:T(8,128)(2,1)S(1)}, u32[]{:S(2)}, u32[]{:S(2)}) %collective-permute-start.8) | collective-permute-done | bytes 65568 | tf_op jit(solution)/shard_map/ppermute | solution.py:262
  58.1 0.6 shard_map.116.w_ref
  58.7 1.4 %shard_map.117 = (bf16[64,4096]{1,0:T(8,128)(2,1)}, bf16[8,4096]{1,0:T(8,128)(2,1)}, bf16[2,128]{1,0:T(2,128)(2,1)}) custom-call(bf16[8,80,512]{2,1,0:T(8,128)(2,1)S(1)} %all-to-all-done.1.y_ref, bf16[8,64,256]{2,1,0:T(8,128)(2,1)S(1)} %shard_map.116.w_ref), custom_call_target="tpu_custom_call" | custom-call | flops 10000000 | bytes 1800000 | tf_op jit(solution)/shard_map/pallas_call | solution.py:279
  (36 shorter events, 0.7 us)
Async XLA Ops:
  1.4 20.2 %collective-permute-start = (bf16[2,256]{1,0:T(2,128)(2,1)S(1)}, bf16[2,256]{1,0:T(2,128)(2,1)S(1)}, u32[]{:S(2)}, u32[]{:S(2)}) collective-permute-start(bf16[2,256]{1,0:T(2,128)(2,1)S(1)} %maximum_maximum_fusion.mine_ref), channel_id=1, source_target_pairs={{0,1},{1,0},{2,3},{3,2},{4,5},{5,4},{6,7},{7,6},{8,9},{9,8},{10,11... | collective-permute-start | bytes 3080 | tf_op jit(solution)/shard_map/ppermute | solution.py:203
  2.8 26.5 %collective-permute-start.3 = (bf16[64,16,128]{2,1,0:T(8,128)(2,1)}, bf16[64,16,128]{2,1,0:T(8,128)(2,1)S(1)}, u32[]{:S(2)}, u32[]{:S(2)}) collective-permute-start(bf16[64,16,128]{2,1,0:T(8,128)(2,1)} %param.14), channel_id=1, source_target_pairs={{0,1},{1,0},{2,3},{3,2},{4,5},{5,4},{6,7},{7,6},{8,9},{9,8},{10,11... | collective-permute-start | bytes 786440 | tf_op jit(solution)/shard_map/ppermute | solution.py:198
  3.1 1.6 %copy-start = (bf16[16,32,2048]{2,1,0:T(8,128)(2,1)S(1)}, bf16[16,32,2048]{2,1,0:T(8,128)(2,1)}, u32[]{:S(2)}) copy-start(bf16[16,32,2048]{2,1,0:T(8,128)(2,1)} %param.9) | copy-start | bytes 6291460
  4.7 1.6 %copy-start.1 = (bf16[2048,512]{1,0:T(8,128)(2,1)S(1)}, bf16[2048,512]{1,0:T(8,128)(2,1)}, u32[]{:S(2)}) copy-start(bf16[2048,512]{1,0:T(8,128)(2,1)} %w_ref.1) | copy-start | bytes 6291460
  6.3 0.9 %copy-start.2 = (bf16[2048,64]{0,1:T(8,128)(2,1)S(1)}, bf16[2048,64]{0,1:T(8,128)(2,1)}, u32[]{:S(2)}) copy-start(bf16[2048,64]{0,1:T(8,128)(2,1)} %param.12) | copy-start | bytes 786436
  7.3 0.7 %copy-start.4 = (f32[2048]{0:T(1024)S(1)}, f32[2048]{0:T(1024)}, u32[]{:S(2)}) copy-start(f32[2048]{0:T(1024)} %param.10) | copy-start | bytes 24580
  8.0 0.7 %copy-start.5 = (f32[512]{0:T(512)S(1)}, f32[512]{0:T(512)}, u32[]{:S(2)}) copy-start(f32[512]{0:T(512)} %param.13) | copy-start | bytes 6148
  11.7 24.5 %all-to-all-start = ((bf16[16,16,1152]{2,1,0:T(8,128)(2,1)}), bf16[16,16,1152]{2,1,0:T(8,128)(2,1)S(1)}, u32[]{:S(2)}, u32[]{:S(2)}) async-start(bf16[16,16,1152]{2,1,0:T(8,128)(2,1)} %shard_map.112), calls=%async_computation | async-start | bytes 1179648 | tf_op jit(solution)/shard_map/all_to_all | solution.py:163
  21.6 7.5 %copy-start.6 = (bf16[64,16,128]{2,1,0:T(8,128)(2,1)S(1)}, bf16[64,16,128]{2,1,0:T(8,128)(2,1)}, u32[]{:S(2)}) copy-start(bf16[64,16,128]{2,1,0:T(8,128)(2,1)} %param.14) | copy-start | bytes 786436
  22.1 4.1 %collective-permute-start.1 = (bf16[16,256]{1,0:T(8,128)(2,1)S(1)}, bf16[16,256]{1,0:T(8,128)(2,1)S(1)}, u32[]{:S(2)}, u32[]{:S(2)}) collective-permute-start(bf16[16,256]{1,0:T(8,128)(2,1)S(1)} %shard_map.113), channel_id=1, source_target_pairs={{0,6},{6,0},{2,4},{4,2},{1,7},{7,1},{3,5},{5,3},{8,14},{14,8},{10,... | collective-permute-start | bytes 24584 | tf_op jit(solution)/shard_map/ppermute | solution.py:212
  26.2 2.8 %collective-permute-start.2 = (bf16[16,256]{1,0:T(8,128)(2,1)S(1)}, bf16[16,256]{1,0:T(8,128)(2,1)S(1)}, u32[]{:S(2)}, u32[]{:S(2)}) collective-permute-start(bf16[16,256]{1,0:T(8,128)(2,1)S(1)} %add.36), channel_id=1, source_target_pairs={{0,2},{2,0},{4,6},{6,4},{1,3},{3,1},{5,7},{7,5},{8,10},{10,8},{12,... | collective-permute-start | bytes 24584 | tf_op jit(solution)/shard_map/ppermute | solution.py:214
  29.3 17.0 %copy-start.3 = (bf16[64,16,128]{2,1,0:T(8,128)(2,1)S(1)}, bf16[64,16,128]{2,1,0:T(8,128)(2,1)}, u32[]{:S(2)}) copy-start(bf16[64,16,128]{2,1,0:T(8,128)(2,1)} %own_ref.1) | copy-start | bytes 786436
  29.7 2.7 %collective-permute-start.4 = (bf16[16,512]{1,0:T(8,128)(2,1)S(1)}, bf16[16,512]{1,0:T(8,128)(2,1)S(1)}, u32[]{:S(2)}, u32[]{:S(2)}) collective-permute-start(bf16[16,512]{1,0:T(8,128)(2,1)S(1)} %fusion.4), channel_id=1, source_target_pairs={{0,2},{2,0},{4,6},{6,4},{1,3},{3,1},{5,7},{7,5},{8,10},{10,8},{12,... | collective-permute-start | bytes 49160 | tf_op jit(solution)/shard_map/ppermute | solution.py:248
  32.4 3.9 %collective-permute-start.5 = (bf16[16,512]{1,0:T(8,128)(2,1)S(1)}, bf16[16,512]{1,0:T(8,128)(2,1)S(1)}, u32[]{:S(2)}, u32[]{:S(2)}) collective-permute-start(bf16[16,512]{1,0:T(8,128)(2,1)S(1)} %fusion.14.a0_ref), channel_id=1, source_target_pairs={{0,6},{6,0},{2,4},{4,2},{1,7},{7,1},{3,5},{5,3},{8,14},{14,8},{10,... | collective-permute-start | bytes 49160 | tf_op jit(solution)/shard_map/ppermute | solution.py:250
  37.7 21.0 %all-to-all-start.1 = ((bf16[8,80,512]{2,1,0:T(8,128)(2,1)}), bf16[8,80,512]{2,1,0:T(8,128)(2,1)S(1)}, u32[]{:S(2)}, u32[]{:S(2)}) async-start(bf16[8,80,512]{2,1,0:T(8,128)(2,1)} %shard_map.114), calls=%async_computation.1 | async-start | bytes 1310720 | tf_op jit(solution)/shard_map/all_to_all | solution.py:163
  46.2 1.7 %collective-permute-start.6 = (bf16[64,16,128]{2,1,0:T(8,128)(2,1)S(1)}, bf16[64,16,128]{2,1,0:T(8,128)(2,1)S(1)}, u32[]{:S(2)}, u32[]{:S(2)}) collective-permute-start(bf16[64,16,128]{2,1,0:T(8,128)(2,1)S(1)} %copy-done.3), channel_id=1, source_target_pairs={{0,1},{1,0},{2,3},{3,2},{4,5},{5,4},{6,7},{7,6},{8,9},{9,8},{10,11... | collective-permute-start | bytes 786440 | tf_op jit(solution)/shard_map/ppermute | solution.py:199
  48.8 7.0 %collective-permute-start.7 = (bf16[2,64,256]{2,1,0:T(8,128)(2,1)S(1)}, bf16[2,64,256]{2,1,0:T(8,128)(2,1)S(1)}, u32[]{:S(2)}, u32[]{:S(2)}) collective-permute-start(bf16[2,64,256]{2,1,0:T(8,128)(2,1)S(1)} %get-tuple-element.11), channel_id=1, source_target_pairs={{0,2},{2,4},{4,6},{6,0},{1,3},{3,5},{5,7},{7,1},{8,10},{10,12},{12... | collective-permute-start | bytes 196616 | tf_op jit(solution)/shard_map/ppermute | solution.py:262
  49.4 8.7 %collective-permute-start.8 = (bf16[2,64,256]{2,1,0:T(8,128)(2,1)S(1)}, bf16[2,64,256]{2,1,0:T(8,128)(2,1)S(1)}, u32[]{:S(2)}, u32[]{:S(2)}) collective-permute-start(bf16[2,64,256]{2,1,0:T(8,128)(2,1)S(1)} %get-tuple-element.12), channel_id=1, source_target_pairs={{0,4},{2,6},{4,0},{6,2},{1,5},{3,7},{5,1},{7,3},{8,12},{10,14},{12... | collective-permute-start | bytes 196616 | tf_op jit(solution)/shard_map/ppermute | solution.py:262
  51.7 6.4 %collective-permute-start.9 = (bf16[2,64,256]{2,1,0:T(8,128)(2,1)S(1)}, bf16[2,64,256]{2,1,0:T(8,128)(2,1)S(1)}, u32[]{:S(2)}, u32[]{:S(2)}) collective-permute-start(bf16[2,64,256]{2,1,0:T(8,128)(2,1)S(1)} %get-tuple-element.13), channel_id=1, source_target_pairs={{0,6},{2,0},{4,2},{6,4},{1,7},{3,1},{5,3},{7,5},{8,14},{10,8},{12,... | collective-permute-start | bytes 196616 | tf_op jit(solution)/shard_map/ppermute | solution.py:262

commit v2 on v1

--- a/solution.py
+++ b/solution.py
@@ -37,23 +37,39 @@
     )
 
 
-def place_queries_kernel(at_ref, mine_ref, partner_ref, out_ref):
-    mine = mine_ref[...].astype(F32)
-    partner = partner_ref[...].astype(F32)
-    first = jnp.where(at_ref[1] == 0, mine, partner)
-    second = jnp.where(at_ref[1] == 0, partner, mine)
+def table_kernel(freq_ref, out_ref):
+    rows, lanes = out_ref.shape[1:]
+    first = lax.axis_index(SP_TP) * rows
+    position = first + lax.broadcasted_iota(jnp.int32, (rows, lanes), 0)
+    angles = position.astype(F32) * freq_ref[...]
+    lane = lax.broadcasted_iota(jnp.int32, (rows, lanes), 1)
+    sin = jnp.sin(angles)
+    out_ref[0] = jnp.cos(angles)
+    out_ref[1] = jnp.where(lane < lanes // 2, -sin, sin)
+
+
+def place_queries_kernel(qn_ref, qr_ref, qn_other_ref, qr_other_ref, out_ref):
+    blank = jnp.zeros(qr_ref.shape, F32)
+    mine = jnp.concatenate([qn_ref[...].astype(F32), qr_ref[...].astype(F32), blank], axis=1)
+    partner = jnp.concatenate(
+        [qn_other_ref[...].astype(F32), qr_other_ref[...].astype(F32), blank], axis=1
+    )
+    core = lax.axis_index("c")
+    first = jnp.where(core == 0, mine, partner)
+    second = jnp.where(core == 0, partner, mine)
     rows = jnp.concatenate([first, second] * 4, axis=0)
     row = lax.broadcasted_iota(jnp.int32, rows.shape, 0) // 4
-    out_ref[...] = jnp.where(row == at_ref[0], rows, 0.0).astype(BF16)
-
-
-def pack_payload_kernel(at_ref, own_ref, other_ref, *refs):
+    out_ref[...] = jnp.where(row == lax.axis_index("x"), rows, 0.0).astype(BF16)
+
+
+def pack_payload_kernel(own_ref, other_ref, *refs):
+    x, core = lax.axis_index("x"), lax.axis_index("c")
     outs, (own_f32, other_f32) = refs[:4], refs[4:]
     heads = own_ref.shape[1]
     own_f32[...] = own_ref[...].astype(F32).reshape(own_f32.shape)
     other_f32[...] = other_ref[...].astype(F32).reshape(other_f32.shape)
     for d, out_ref in enumerate(outs):
-        first = 2 * (2 * ((at_ref[0] + d) % 4) + at_ref[1])
+        first = 2 * (2 * ((x + d) % 4) + core)
         for r, source in enumerate((own_f32, other_f32)):
             for h in range(2):
                 rows = source[pl.ds(first + h, out_ref.shape[1], stride=heads), :]
@@ -117,11 +133,12 @@
         out_ref[slot, 64:80, :] = block.astype(BF16)
 
 
-def order_payload_kernel(at_ref, p0_ref, p1_ref, p2_ref, p3_ref, out_ref):
+def order_payload_kernel(p0_ref, p1_ref, p2_ref, p3_ref, out_ref):
+    x, core = lax.axis_index("x"), lax.axis_index("c")
     for d, piece in enumerate((p0_ref, p1_ref, p2_ref, p3_ref)):
-        chip = (at_ref[0] + 4 - d) % 4
-        out_ref[2 * chip + at_ref[1]] = piece[0]
-        out_ref[2 * chip + 1 - at_ref[1]] = piece[1]
+        chip = (x + 4 - d) % 4
+        out_ref[2 * chip + core] = piece[0]
+        out_ref[2 * chip + 1 - core] = piece[1]
 
 
 def finish_kernel(y_ref, w_ref, st_ref, rt_ref, fr_ref):
@@ -187,38 +204,31 @@
     seqs, pos_local, width = layer_input.shape
     tp = lax.axis_size(TP)
     sp = lax.axis_size("sp")
-    block = lax.axis_index(SP_TP)
     shape = jax.ShapeDtypeStruct
 
-    at = jnp.stack([lax.axis_index("x"), lax.axis_index("c")]).astype(jnp.int32)
-    small = pl.BlockSpec(memory_space=pltpu.SMEM)
-    whole = pl.BlockSpec(memory_space=pltpu.VMEM)
-    outside = pl.BlockSpec(memory_space=pltpu.HBM)
+    at = (lax.axis_index("x"), lax.axis_index("c"))
     swap = [(0, 1), (1, 0)]
     lookup_other = lax.ppermute(lookup_widening, "c", swap)
     payload_other = lax.ppermute(payload_widening, "c", swap)
-    mine = jnp.concatenate(
-        [query_nope[0], query_rotary[0], jnp.zeros_like(query_rotary[0])], axis=1
-    )
-    partner = lax.ppermute(mine, "c", swap)
+    nope_other = lax.ppermute(query_nope[0], "c", swap)
+    rotary_other = lax.ppermute(query_rotary[0], "c", swap)
+    table = call(
+        table_kernel,
+        shape((2, pos_local, QK_ROPE), F32),
+        30_000_000_000,
+        60_000_000,
+    )(jnp.tile(frequencies(), 2)[None])
     query = call(
         place_queries_kernel,
         shape((2 * tp, 256), BF16),
-        30_000_000_000,
-        60_000_000,
-        in_specs=[small, whole, whole],
-    )(at, mine, partner)
+        1_000_000,
+        10_000,
+    )(query_nope[0], query_rotary[0], nope_other, rotary_other)
     near, far = [(0, 1), (1, 0), (2, 3), (3, 2)], [(0, 3), (3, 0), (1, 2), (2, 1)]
     moved = lax.ppermute(query, "x", far)
     query = query + moved
     moved = lax.ppermute(query, "x", near)
 
-    positions = (block * pos_local + jnp.arange(pos_local, dtype=jnp.int32)).astype(F32)
-    angles = positions[:, None] * frequencies()[None, :]
-    cos, sin = jnp.cos(angles), jnp.sin(angles)
-    table = jnp.stack(
-        [jnp.concatenate([cos, cos], axis=1), jnp.concatenate([-sin, sin], axis=1)]
-    )
     sent = call(
         project_kernel,
         shape((seqs, pos_local // 2, 1152), BF16),
@@ -254,9 +264,8 @@
         [shape((2, each, 256), BF16)] * 4,
         1_000_000,
         1_000_000,
-        in_specs=[small, whole, whole],
         scratch_shapes=[pltpu.VMEM((each * 2 * tp, 128), F32)] * 2,
-    )(at, payload_widening, payload_other)
+    )(payload_widening, payload_other)
     pieces = [parts[0]]
     for d in (1, 2, 3):
         pieces.append(lax.ppermute(parts[d], "x", [(i, (i + d) % 4) for i in range(4)]))
@@ -267,13 +276,7 @@
         held, placed, other, turned
     )
     arrived = exchange(piece, sp, tp, False)
-    weight = call(
-        order_payload_kernel,
-        shape((tp, each, 256), BF16),
-        1_000_000,
-        500_000,
-        in_specs=[small] + [whole] * 4,
-    )(at, *pieces)
+    weight = call(order_payload_kernel, shape((tp, each, 256), BF16), 1_000_000, 500_000)(*pieces)
 
     total = sp * tp * pos_local
     stored, rotary, first = call(

time: 60.6 us -> 55.3 us (0.913)
  local copies, waits for them, and re-layouts: 5.7 us -> 2.35 us
  Pallas kernels: 7.8 us -> 6.3 us
  other arithmetic: 1.27 us -> 0.28 us
  waiting for transfers between devices: 15.4 us -> 16.2 us
    unnamed x14 -> x18, local copies, waits for them, and re-layouts: 5.51 us -> 2.15 us
    pallas_call x2 -> x3, Pallas kernels: 1.12 us -> 0.14 us  [the longest x1 0.09 us: shards(): call(table_kernel, shape((2, pos_local, QK_ROPE), F32), 30000000000, 6000...]
    ppermute x3, waiting for transfers between devices: 6.04 us -> 6.87 us  [shards(): lax.ppermute(parts[d], 'x', [(i, (i + d) % 4) for i in range(4)])]
    concatenate x1 -> x0, other arithmetic: 0.68 us -> none  [shards(): jnp.concatenate([query_nope[0], query_rotary[0], jnp.zeros_like(query_rot...]
    ppermute x1 -> x2, starting transfers between devices: 1.38 us -> 1.56 us  [the longest x1 1.46 us: shards(): nope_other = lax.ppermute(query_nope[0], 'c', swap)]
  transfers between devices with their start and end apart: 12 -> 13, of which waited for: 7 -> 8; matrix products, arithmetic and copies ran while one was open for 2% -> 2% of each run, Pallas kernels for 8% -> 6%
where the time goes in v2:
time: 55.3 us; the launch traced here: 55 us
  starting transfers between devices  28.6 us (52%)
  waiting for transfers between devices  16.2 us (29%)
  Pallas kernels  6.3 us (11%)
  local copies, waits for them, and re-layouts  2.35 us (4%)
  between operations  0.78 us (1%)
    all_to_all x2, starting transfers between devices, exchange(): lax.all_to_all(array, SP_TP, 0, 0, tiled=True, axis_index_groups=groups)  18 us
    ppermute x3, waiting for transfers between devices, shards(): lax.ppermute(parts[d], 'x', [(i, (i + d) % 4) for i in range(4)])  6.87 us
    pallas_call x1, Pallas kernels, shards(): call(project_kernel, shape((seqs, pos_local // 2, 1152), BF16), 130000000...  3.08 us
    ppermute x3, starting transfers between devices, shards(): lax.ppermute(parts[d], 'x', [(i, (i + d) % 4) for i in range(4)])  3.03 us
    ppermute x1, waiting for transfers between devices, shards(): moved = lax.ppermute(query, 'x', near)  2.78 us
    ppermute x1, starting transfers between devices, shards(): moved = lax.ppermute(query, 'x', far)  2.56 us
    ppermute x1, starting transfers between devices, shards(): other = lax.ppermute(placed, 'x', far)  2.56 us
    ppermute x1, waiting for transfers between devices, shards(): moved = lax.ppermute(placed, 'x', near)  2.5 us
  transfers between devices with their start and end apart: 13, of which 8 were waited for; matrix products, arithmetic and copies ran while one was open for 2% of the time, Pallas kernels for 6%

profile of v2, /device:TPU:1, one launch (start us, length us, event | category | flops | bytes accessed | tf_op | source)
XLA Modules:
  0.0 55.0 jit_solution(1101238057804103605)
XLA Ops:
  0.6 1.5 %collective-permute-start = (bf16[2,128]{1,0:T(2,128)(2,1)}, bf16[2,128]{1,0:T(2,128)(2,1)S(1)}, u32[]{:S(2)}, u32[]{:S(2)}) collective-permute-start(bf16[2,128]{1,0:T(2,128)(2,1)} %bitcast.23), channel_id=1, source_target_pairs={{0,1},{1,0},{2,3},{3,2},{4,5},{5,4},{6,7},{7,6},{8,9},{9,8},{10,11... | collective-permute-start | bytes 1544 | tf_op jit(solution)/shard_map/ppermute | solution.py:213
  2.1 0.1 collective-permute-start.1
  2.2 0.4 collective-permute-start.4
  2.6 0.1 broadcast_in_dim_tile.3.freq_ref
  2.7 0.1 shard_map.112.cs_ref
  2.8 1.5 %copy-done = bf16[16,32,2048]{2,1,0:T(8,128)(2,1)S(1)} copy-done((bf16[16,32,2048]{2,1,0:T(8,128)(2,1)S(1)}, bf16[16,32,2048]{2,1,0:T(8,128)(2,1)}, u32[]{:S(2)}) %copy-start) | copy-done | bytes 2097176
  4.3 0.6 %copy-done.1 = bf16[2048,512]{1,0:T(8,128)(2,1)S(1)} copy-done((bf16[2048,512]{1,0:T(8,128)(2,1)S(1)}, bf16[2048,512]{1,0:T(8,128)(2,1)}, u32[]{:S(2)}) %copy-start.1) | copy-done | bytes 2097176
  5.0 3.1 %shard_map.113 = bf16[16,16,1152]{2,1,0:T(8,128)(2,1)} custom-call(bf16[512,2048]{1,0:T(8,128)(2,1)S(1)} %bitcast.19, f32[1,2048]{1,0:T(1,128)S(1)} %bitcast.21, bf16[2048,512]{1,0:T(8,128)(2,1)S(1)} %copy-done.1, bf16[64,2048]{1,0:T(8,128)(2,1)S(1)} %bitcast.20, f32[1,512]{1,0:T(1,128)S(1)} %bitcast.22, f32[2,32,64]{2,1,0:T(8,128)S(1)} %shard_map.112.cs_ref), custom_call_target="tpu_custom_call" | custom-call | flops 1300000000 | bytes 5000000 | tf_op jit(solution)/shard_map/pallas_call | solution.py:232
  8.1 9.8 %all-to-all-start = ((bf16[16,16,1152]{2,1,0:T(8,128)(2,1)}), bf16[16,16,1152]{2,1,0:T(8,128)(2,1)S(1)}, u32[]{:S(2)}, u32[]{:S(2)}) async-start(bf16[16,16,1152]{2,1,0:T(8,128)(2,1)} %shard_map.113), calls=%async_computation | async-start | bytes 1179648 | tf_op jit(solution)/shard_map/all_to_all | solution.py:180
  17.9 2.6 %collective-permute-start.2 = (bf16[16,256]{1,0:T(8,128)(2,1)S(1)}, bf16[16,256]{1,0:T(8,128)(2,1)S(1)}, u32[]{:S(2)}, u32[]{:S(2)}) collective-permute-start(bf16[16,256]{1,0:T(8,128)(2,1)S(1)} %shard_map.114), channel_id=1, source_target_pairs={{0,6},{6,0},{2,4},{4,2},{1,7},{7,1},{3,5},{5,3},{8,14},{14,8},{10,... | collective-permute-start | bytes 24584 | tf_op jit(solution)/shard_map/ppermute | solution.py:228
  20.5 1.5 %collective-permute-done.2 = bf16[16,256]{1,0:T(8,128)(2,1)S(1)} collective-permute-done((bf16[16,256]{1,0:T(8,128)(2,1)S(1)}, bf16[16,256]{1,0:T(8,128)(2,1)S(1)}, u32[]{:S(2)}, u32[]{:S(2)}) %collective-permute-start.2) | collective-permute-done | bytes 8224 | tf_op jit(solution)/shard_map/ppermute | solution.py:228
  22.0 2.8 %collective-permute-done.3 = bf16[16,256]{1,0:T(8,128)(2,1)S(1)} collective-permute-done((bf16[16,256]{1,0:T(8,128)(2,1)S(1)}, bf16[16,256]{1,0:T(8,128)(2,1)S(1)}, u32[]{:S(2)}, u32[]{:S(2)}) %collective-permute-start.3) | collective-permute-done | bytes 8224 | tf_op jit(solution)/shard_map/ppermute | solution.py:230
  24.8 0.2 fusion.2
  25.1 0.3 fusion
  25.3 0.1 concatenate.10
  25.5 0.1 collective-permute-start.5
  25.5 0.1 subtract_convert_fusion
  25.6 2.5 %collective-permute-done.5 = bf16[16,512]{1,0:T(8,128)(2,1)S(1)} collective-permute-done((bf16[16,512]{1,0:T(8,128)(2,1)S(1)}, bf16[16,512]{1,0:T(8,128)(2,1)S(1)}, u32[]{:S(2)}, u32[]{:S(2)}) %collective-permute-start.5) | collective-permute-done | bytes 16416 | tf_op jit(solution)/shard_map/ppermute | solution.py:258
  28.1 2.6 %collective-permute-start.6 = (bf16[16,512]{1,0:T(8,128)(2,1)S(1)}, bf16[16,512]{1,0:T(8,128)(2,1)S(1)}, u32[]{:S(2)}, u32[]{:S(2)}) collective-permute-start(bf16[16,512]{1,0:T(8,128)(2,1)S(1)} %fusion.13.a0_ref), channel_id=1, source_target_pairs={{0,6},{6,0},{2,4},{4,2},{1,7},{7,1},{3,5},{5,3},{8,14},{14,8},{10,... | collective-permute-start | bytes 49160 | tf_op jit(solution)/shard_map/ppermute | solution.py:260
  30.7 0.1 fusion.9.t_ref
  30.8 1.2 %collective-permute-done.6.a1_ref = bf16[16,512]{1,0:T(8,128)(2,1)S(1)} collective-permute-done((bf16[16,512]{1,0:T(8,128)(2,1)S(1)}, bf16[16,512]{1,0:T(8,128)(2,1)S(1)}, u32[]{:S(2)}, u32[]{:S(2)}) %collective-permute-start.6) | collective-permute-done | bytes 16416 | tf_op jit(solution)/shard_map/ppermute | solution.py:260
  32.0 1.4 %shard_map.115 = bf16[8,80,512]{2,1,0:T(8,128)(2,1)} custom-call(bf16[16,16,1152]{2,1,0:T(8,128)(2,1)S(1)} %all-to-all-done.z_ref, bf16[16,512]{1,0:T(8,128)(2,1)S(1)} %fusion.13.a0_ref, bf16[16,512]{1,0:T(8,128)(2,1)S(1)} %collective-permute-done.6.a1_ref, bf16[16,128]{1,0:T(8,128)(2,1)S(1)} %fusion.9.t_ref), custom_call_target="tpu_custom_call" | custom-call | flops 600000000 | bytes 1300000 | tf_op jit(solution)/shard_map/pallas_call | solution.py:275
  33.5 8.2 %all-to-all-start.1 = ((bf16[8,80,512]{2,1,0:T(8,128)(2,1)}), bf16[8,80,512]{2,1,0:T(8,128)(2,1)S(1)}, u32[]{:S(2)}, u32[]{:S(2)}) async-start(bf16[8,80,512]{2,1,0:T(8,128)(2,1)} %shard_map.115), calls=%async_computation.1 | async-start | bytes 1310720 | tf_op jit(solution)/shard_map/all_to_all | solution.py:180
  41.7 0.4 collective-permute-start.7
  42.1 1.3 %collective-permute-done.7.other_ref = bf16[64,16,128]{2,1,0:T(8,128)(2,1)S(1)} collective-permute-done((bf16[64,16,128]{2,1,0:T(8,128)(2,1)S(1)}, bf16[64,16,128]{2,1,0:T(8,128)(2,1)S(1)}, u32[]{:S(2)}, u32[]{:S(2)}) %collective-permute-start.7) | collective-permute-done | bytes 262176 | tf_op jit(solution)/shard_map/ppermute | solution.py:212
  43.4 0.2 shard_map.116
  43.7 1.8 %collective-permute-start.10 = (bf16[2,64,256]{2,1,0:T(8,128)(2,1)S(1)}, bf16[2,64,256]{2,1,0:T(8,128)(2,1)S(1)}, u32[]{:S(2)}, u32[]{:S(2)}) collective-permute-start(bf16[2,64,256]{2,1,0:T(8,128)(2,1)S(1)} %get-tuple-element.13), channel_id=1, source_target_pairs={{0,6},{2,0},{4,2},{6,4},{1,7},{3,1},{5,3},{7,5},{8,14},{10,8},{12,... | collective-permute-start | bytes 196616 | tf_op jit(solution)/shard_map/ppermute | solution.py:271
  45.4 1.3 %collective-permute-start.9 = (bf16[2,64,256]{2,1,0:T(8,128)(2,1)S(1)}, bf16[2,64,256]{2,1,0:T(8,128)(2,1)S(1)}, u32[]{:S(2)}, u32[]{:S(2)}) collective-permute-start(bf16[2,64,256]{2,1,0:T(8,128)(2,1)S(1)} %get-tuple-element.12), channel_id=1, source_target_pairs={{0,4},{2,6},{4,0},{6,2},{1,5},{3,7},{5,1},{7,3},{8,12},{10,14},{12... | collective-permute-start | bytes 196616 | tf_op jit(solution)/shard_map/ppermute | solution.py:271
  46.7 4.9 %collective-permute-done.10.p3_ref = bf16[2,64,256]{2,1,0:T(8,128)(2,1)S(1)} collective-permute-done((bf16[2,64,256]{2,1,0:T(8,128)(2,1)S(1)}, bf16[2,64,256]{2,1,0:T(8,128)(2,1)S(1)}, u32[]{:S(2)}, u32[]{:S(2)}) %collective-permute-start.10) | collective-permute-done | bytes 65568 | tf_op jit(solution)/shard_map/ppermute | solution.py:271
  51.6 0.2 collective-permute-done.8.p1_ref
  51.8 1.8 %collective-permute-done.9.p2_ref = bf16[2,64,256]{2,1,0:T(8,128)(2,1)S(1)} collective-permute-done((bf16[2,64,256]{2,1,0:T(8,128)(2,1)S(1)}, bf16[2,64,256]{2,1,0:T(8,128)(2,1)S(1)}, u32[]{:S(2)}, u32[]{:S(2)}) %collective-permute-start.9) | collective-permute-done | bytes 65568 | tf_op jit(solution)/shard_map/ppermute | solution.py:271
  53.6 1.4 %shard_map.118 = (bf16[64,4096]{1,0:T(8,128)(2,1)}, bf16[8,4096]{1,0:T(8,128)(2,1)}, bf16[2,128]{1,0:T(2,128)(2,1)}) custom-call(bf16[8,80,512]{2,1,0:T(8,128)(2,1)S(1)} %all-to-all-done.1.y_ref, bf16[8,64,256]{2,1,0:T(8,128)(2,1)S(1)} %shard_map.117.w_ref), custom_call_target="tpu_custom_call" | custom-call | flops 10000000 | bytes 1800000 | tf_op jit(solution)/shard_map/pallas_call | solution.py:282
  (37 shorter events, 0.2 us)
Async XLA Ops:
  0.6 17.2 %collective-permute-start = (bf16[2,128]{1,0:T(2,128)(2,1)}, bf16[2,128]{1,0:T(2,128)(2,1)S(1)}, u32[]{:S(2)}, u32[]{:S(2)}) collective-permute-start(bf16[2,128]{1,0:T(2,128)(2,1)} %bitcast.23), channel_id=1, source_target_pairs={{0,1},{1,0},{2,3},{3,2},{4,5},{5,4},{6,7},{7,6},{8,9},{9,8},{10,11... | collective-permute-start | bytes 1544 | tf_op jit(solution)/shard_map/ppermute | solution.py:213
  2.1 15.8 %collective-permute-start.1 = (bf16[2,64]{1,0:T(2,128)(2,1)}, bf16[2,64]{1,0:T(2,128)(2,1)S(1)}, u32[]{:S(2)}, u32[]{:S(2)}) collective-permute-start(bf16[2,64]{1,0:T(2,128)(2,1)} %bitcast.25), channel_id=1, source_target_pairs={{0,1},{1,0},{2,3},{3,2},{4,5},{5,4},{6,7},{7,6},{8,9},{9,8},{10,11... | collective-permute-start | bytes 776 | tf_op jit(solution)/shard_map/ppermute | solution.py:214
  2.2 22.9 %collective-permute-start.4 = (bf16[64,16,128]{2,1,0:T(8,128)(2,1)}, bf16[64,16,128]{2,1,0:T(8,128)(2,1)S(1)}, u32[]{:S(2)}, u32[]{:S(2)}) collective-permute-start(bf16[64,16,128]{2,1,0:T(8,128)(2,1)} %param.14), channel_id=1, source_target_pairs={{0,1},{1,0},{2,3},{3,2},{4,5},{5,4},{6,7},{7,6},{8,9},{9,8},{10,11... | collective-permute-start | bytes 786440 | tf_op jit(solution)/shard_map/ppermute | solution.py:211
  2.7 1.6 %copy-start = (bf16[16,32,2048]{2,1,0:T(8,128)(2,1)S(1)}, bf16[16,32,2048]{2,1,0:T(8,128)(2,1)}, u32[]{:S(2)}) copy-start(bf16[16,32,2048]{2,1,0:T(8,128)(2,1)} %param.9) | copy-start | bytes 6291460
  2.7 2.2 %copy-start.1 = (bf16[2048,512]{1,0:T(8,128)(2,1)S(1)}, bf16[2048,512]{1,0:T(8,128)(2,1)}, u32[]{:S(2)}) copy-start(bf16[2048,512]{1,0:T(8,128)(2,1)} %w_ref.1) | copy-start | bytes 6291460
  2.7 2.2 %copy-start.2 = (bf16[2048,64]{0,1:T(8,128)(2,1)S(1)}, bf16[2048,64]{0,1:T(8,128)(2,1)}, u32[]{:S(2)}) copy-start(bf16[2048,64]{0,1:T(8,128)(2,1)} %param.12) | copy-start | bytes 786436
  2.7 2.2 %copy-start.4 = (f32[2048]{0:T(1024)S(1)}, f32[2048]{0:T(1024)}, u32[]{:S(2)}) copy-start(f32[2048]{0:T(1024)} %param.10) | copy-start | bytes 24580
  2.7 2.2 %copy-start.5 = (f32[512]{0:T(512)S(1)}, f32[512]{0:T(512)}, u32[]{:S(2)}) copy-start(f32[512]{0:T(512)} %param.13) | copy-start | bytes 6148
  4.9 12.9 %copy-start.6 = (bf16[1,2,128]{2,1,0:T(2,128)(2,1)S(1)}, bf16[1,2,128]{2,1,0:T(2,128)(2,1)}, u32[]{:S(2)}) copy-start(bf16[1,2,128]{2,1,0:T(2,128)(2,1)} %param.16) | copy-start | bytes 1540
  4.9 12.9 %copy-start.7 = (bf16[1,2,64]{2,1,0:T(2,128)(2,1)S(1)}, bf16[1,2,64]{2,1,0:T(2,128)(2,1)}, u32[]{:S(2)}) copy-start(bf16[1,2,64]{2,1,0:T(2,128)(2,1)} %param.17) | copy-start | bytes 772
  5.0 19.9 %copy-start.8 = (bf16[64,16,128]{2,1,0:T(8,128)(2,1)S(1)}, bf16[64,16,128]{2,1,0:T(8,128)(2,1)}, u32[]{:S(2)}) copy-start(bf16[64,16,128]{2,1,0:T(8,128)(2,1)} %param.14) | copy-start | bytes 786436
  8.1 24.0 %all-to-all-start = ((bf16[16,16,1152]{2,1,0:T(8,128)(2,1)}), bf16[16,16,1152]{2,1,0:T(8,128)(2,1)S(1)}, u32[]{:S(2)}, u32[]{:S(2)}) async-start(bf16[16,16,1152]{2,1,0:T(8,128)(2,1)} %shard_map.113), calls=%async_computation | async-start | bytes 1179648 | tf_op jit(solution)/shard_map/all_to_all | solution.py:180
  17.9 4.1 %collective-permute-start.2 = (bf16[16,256]{1,0:T(8,128)(2,1)S(1)}, bf16[16,256]{1,0:T(8,128)(2,1)S(1)}, u32[]{:S(2)}, u32[]{:S(2)}) collective-permute-start(bf16[16,256]{1,0:T(8,128)(2,1)S(1)} %shard_map.114), channel_id=1, source_target_pairs={{0,6},{6,0},{2,4},{4,2},{1,7},{7,1},{3,5},{5,3},{8,14},{14,8},{10,... | collective-permute-start | bytes 24584 | tf_op jit(solution)/shard_map/ppermute | solution.py:228
  22.0 2.8 %collective-permute-start.3 = (bf16[16,256]{1,0:T(8,128)(2,1)S(1)}, bf16[16,256]{1,0:T(8,128)(2,1)S(1)}, u32[]{:S(2)}, u32[]{:S(2)}) collective-permute-start(bf16[16,256]{1,0:T(8,128)(2,1)S(1)} %add.16), channel_id=1, source_target_pairs={{0,2},{2,0},{4,6},{6,4},{1,3},{3,1},{5,7},{7,5},{8,10},{10,8},{12,... | collective-permute-start | bytes 24584 | tf_op jit(solution)/shard_map/ppermute | solution.py:230
  25.1 16.6 %copy-start.3 = (bf16[64,16,128]{2,1,0:T(8,128)(2,1)S(1)}, bf16[64,16,128]{2,1,0:T(8,128)(2,1)}, u32[]{:S(2)}) copy-start(bf16[64,16,128]{2,1,0:T(8,128)(2,1)} %own_ref.1) | copy-start | bytes 786436
  25.5 2.7 %collective-permute-start.5 = (bf16[16,512]{1,0:T(8,128)(2,1)S(1)}, bf16[16,512]{1,0:T(8,128)(2,1)S(1)}, u32[]{:S(2)}, u32[]{:S(2)}) collective-permute-start(bf16[16,512]{1,0:T(8,128)(2,1)S(1)} %fusion.4), channel_id=1, source_target_pairs={{0,2},{2,0},{4,6},{6,4},{1,3},{3,1},{5,7},{7,5},{8,10},{10,8},{12,... | collective-permute-start | bytes 49160 | tf_op jit(solution)/shard_map/ppermute | solution.py:258
  28.1 3.9 %collective-permute-start.6 = (bf16[16,512]{1,0:T(8,128)(2,1)S(1)}, bf16[16,512]{1,0:T(8,128)(2,1)S(1)}, u32[]{:S(2)}, u32[]{:S(2)}) collective-permute-start(bf16[16,512]{1,0:T(8,128)(2,1)S(1)} %fusion.13.a0_ref), channel_id=1, source_target_pairs={{0,6},{6,0},{2,4},{4,2},{1,7},{7,1},{3,5},{5,3},{8,14},{14,8},{10,... | collective-permute-start | bytes 49160 | tf_op jit(solution)/shard_map/ppermute | solution.py:260
  33.5 20.1 %all-to-all-start.1 = ((bf16[8,80,512]{2,1,0:T(8,128)(2,1)}), bf16[8,80,512]{2,1,0:T(8,128)(2,1)S(1)}, u32[]{:S(2)}, u32[]{:S(2)}) async-start(bf16[8,80,512]{2,1,0:T(8,128)(2,1)} %shard_map.115), calls=%async_computation.1 | async-start | bytes 1310720 | tf_op jit(solution)/shard_map/all_to_all | solution.py:180
  41.7 1.7 %collective-permute-start.7 = (bf16[64,16,128]{2,1,0:T(8,128)(2,1)S(1)}, bf16[64,16,128]{2,1,0:T(8,128)(2,1)S(1)}, u32[]{:S(2)}, u32[]{:S(2)}) collective-permute-start(bf16[64,16,128]{2,1,0:T(8,128)(2,1)S(1)} %copy-done.3), channel_id=1, source_target_pairs={{0,1},{1,0},{2,3},{3,2},{4,5},{5,4},{6,7},{7,6},{8,9},{9,8},{10,11... | collective-permute-start | bytes 786440 | tf_op jit(solution)/shard_map/ppermute | solution.py:212
  43.7 7.9 %collective-permute-start.10 = (bf16[2,64,256]{2,1,0:T(8,128)(2,1)S(1)}, bf16[2,64,256]{2,1,0:T(8,128)(2,1)S(1)}, u32[]{:S(2)}, u32[]{:S(2)}) collective-permute-start(bf16[2,64,256]{2,1,0:T(8,128)(2,1)S(1)} %get-tuple-element.13), channel_id=1, source_target_pairs={{0,6},{2,0},{4,2},{6,4},{1,7},{3,1},{5,3},{7,5},{8,14},{10,8},{12,... | collective-permute-start | bytes 196616 | tf_op jit(solution)/shard_map/ppermute | solution.py:271
  45.4 6.3 %collective-permute-start.8 = (bf16[2,64,256]{2,1,0:T(8,128)(2,1)S(1)}, bf16[2,64,256]{2,1,0:T(8,128)(2,1)S(1)}, u32[]{:S(2)}, u32[]{:S(2)}) collective-permute-start(bf16[2,64,256]{2,1,0:T(8,128)(2,1)S(1)} %get-tuple-element.11), channel_id=1, source_target_pairs={{0,2},{2,4},{4,6},{6,0},{1,3},{3,5},{5,7},{7,1},{8,10},{10,12},{12... | collective-permute-start | bytes 196616 | tf_op jit(solution)/shard_map/ppermute | solution.py:271
  45.4 8.1 %collective-permute-start.9 = (bf16[2,64,256]{2,1,0:T(8,128)(2,1)S(1)}, bf16[2,64,256]{2,1,0:T(8,128)(2,1)S(1)}, u32[]{:S(2)}, u32[]{:S(2)}) collective-permute-start(bf16[2,64,256]{2,1,0:T(8,128)(2,1)S(1)} %get-tuple-element.12), channel_id=1, source_target_pairs={{0,4},{2,6},{4,0},{6,2},{1,5},{3,7},{5,1},{7,3},{8,12},{10,14},{12... | collective-permute-start | bytes 196616 | tf_op jit(solution)/shard_map/ppermute | solution.py:271

commit v3 on v2

--- a/solution.py
+++ b/solution.py
@@ -62,9 +62,11 @@
     out_ref[...] = jnp.where(row == lax.axis_index("x"), rows, 0.0).astype(BF16)
 
 
-def pack_payload_kernel(own_ref, other_ref, *refs):
+def pack_payload_kernel(share_ref, own_ref, other_ref, *refs):
     x, core = lax.axis_index("x"), lax.axis_index("c")
     outs, (own_f32, other_f32) = refs[:4], refs[4:]
+    each = own_ref.shape[0]
+    absorbed = jnp.concatenate([share_ref[...], jnp.zeros_like(share_ref)], axis=1)
     heads = own_ref.shape[1]
     own_f32[...] = own_ref[...].astype(F32).reshape(own_f32.shape)
     other_f32[...] = other_ref[...].astype(F32).reshape(other_f32.shape)
@@ -72,8 +74,9 @@
         first = 2 * (2 * ((x + d) % 4) + core)
         for r, source in enumerate((own_f32, other_f32)):
             for h in range(2):
-                rows = source[pl.ds(first + h, out_ref.shape[1], stride=heads), :]
-                out_ref[r, :, h * 128 : (h + 1) * 128] = rows.astype(BF16)
+                rows = source[pl.ds(first + h, each, stride=heads), :]
+                out_ref[r, 0:each, h * 128 : (h + 1) * 128] = rows.astype(BF16)
+            out_ref[r, each:, :] = absorbed
 
 
 def project_kernel(x_ref, gain_ref, w_ref, r_ref, scal_ref, cs_ref, out_ref):
@@ -100,7 +103,13 @@
         out_ref[slot, :, 1024:1152] = pair.astype(BF16)
 
 
-def attend_kernel(z_ref, a0_ref, a1_ref, t_ref, out_ref):
+def attend_kernel(z_ref, p0_ref, p1_ref, p2_ref, p3_ref, t_ref, out_ref, w_ref, a_ref):
+    core = lax.axis_index("c")
+    for d, piece in enumerate((p0_ref, p1_ref, p2_ref, p3_ref)):
+        chip = (lax.axis_index("x") + 4 - d) % 4
+        a_ref[:, pl.ds(pl.multiple_of(chip * 128, 128), 128)] = piece[0, 64:80, 0:128]
+        w_ref[2 * chip + core] = piece[0, 0:64]
+        w_ref[2 * chip + 1 - core] = piece[1, 0:64]
     lats, rots = [], []
     for i in range(z_ref.shape[0] - 1, -1, -1):
         lats += [z_ref[i, :, 0:512], z_ref[i, :, 512:1024]]
@@ -108,7 +117,7 @@
         rots += [pair, jnp.concatenate([pair[:, 64:], pair[:, :64]], axis=1)]
     lat = jnp.concatenate(lats, axis=0)
     rot = jnp.concatenate(rots, axis=0)
-    absorbed = a0_ref[...] + a1_ref[...]
+    absorbed = a_ref[...]
     scores = lax.dot_general(absorbed, lat, LAST, preferred_element_type=F32)
     scores = scores + lax.dot_general(t_ref[...], rot, LAST, preferred_element_type=F32)
     scores = scores * ((PLAIN_MATCH_SPAN + QK_ROPE) ** (-0.5))
@@ -131,14 +140,6 @@
             [rot_t[8 * t : 8 * t + 8], context[mine], top[mine], high[mine], low[mine]], axis=0
         )
         out_ref[slot, 64:80, :] = block.astype(BF16)
-
-
-def order_payload_kernel(p0_ref, p1_ref, p2_ref, p3_ref, out_ref):
-    x, core = lax.axis_index("x"), lax.axis_index("c")
-    for d, piece in enumerate((p0_ref, p1_ref, p2_ref, p3_ref)):
-        chip = (x + 4 - d) % 4
-        out_ref[2 * chip + core] = piece[0]
-        out_ref[2 * chip + 1 - core] = piece[1]
 
 
 def finish_kernel(y_ref, w_ref, st_ref, rt_ref, fr_ref):
@@ -252,32 +253,29 @@
         for weight in (lookup_widening, lookup_other)
     )
     first, second = jnp.where(at[1] == 0, own, partner), jnp.where(at[1] == 0, partner, own)
-    share = jnp.concatenate([first, second] * 4, axis=1)
-    lane = lax.broadcasted_iota(jnp.int32, (2 * tp, 512), 1) // 128
-    placed = jnp.where(lane == at[0], share, jnp.zeros((), BF16))
-    moved = lax.ppermute(placed, "x", near)
-    placed = placed + moved
-    other = lax.ppermute(placed, "x", far)
+    share = jnp.concatenate([first, second], axis=1)
     each = payload_widening.shape[0]
     parts = call(
         pack_payload_kernel,
-        [shape((2, each, 256), BF16)] * 4,
+        [shape((2, each + 2 * tp, 256), BF16)] * 4,
         1_000_000,
         1_000_000,
         scratch_shapes=[pltpu.VMEM((each * 2 * tp, 128), F32)] * 2,
-    )(payload_widening, payload_other)
+    )(share, payload_widening, payload_other)
     pieces = [parts[0]]
     for d in (1, 2, 3):
         pieces.append(lax.ppermute(parts[d], "x", [(i, (i + d) % 4) for i in range(4)]))
     turned = rotate(turn.astype(F32), F32(seqs * 0 + sp * tp * pos_local)).astype(BF16)
     turned = jnp.concatenate([turned, jnp.zeros_like(turned)], axis=1)
 
-    piece = call(attend_kernel, shape((tp, 80, 512), BF16), 600_000_000, 1_300_000)(
-        held, placed, other, turned
-    )
+    piece, weight = call(
+        attend_kernel,
+        (shape((tp, 80, 512), BF16), shape((tp, each, 256), BF16)),
+        600_000_000,
+        1_300_000,
+        scratch_shapes=[pltpu.VMEM((2 * tp, 512), BF16)],
+    )(held, *pieces, turned)
     arrived = exchange(piece, sp, tp, False)
-    weight = call(order_payload_kernel, shape((tp, each, 256), BF16), 1_000_000, 500_000)(*pieces)
-
     total = sp * tp * pos_local
     stored, rotary, first = call(
         finish_kernel,

time: 55.3 us -> 47.6 us (0.86)
  blocking collectives: 0 us -> 16.1 us
  waiting for transfers between devices: 16.2 us -> 5.36 us
  starting transfers between devices: 28.6 us -> 18.7 us
  local copies, waits for them, and re-layouts: 2.35 us -> 0.21 us
  Pallas kernels: 6.3 us -> 5.45 us
    all_to_all x0 -> x1, blocking collectives: none -> 16.1 us  [exchange(): lax.all_to_all(array, SP_TP, 0, 0, tiled=True, axis_index_groups=groups)]
    all_to_all x2 -> x1, starting transfers between devices: 18 us -> 9.81 us  [exchange(): lax.all_to_all(array, SP_TP, 0, 0, tiled=True, axis_index_groups=groups)]
    ppermute x3, waiting for transfers between devices: 6.87 us -> 2.36 us  [shards(): lax.ppermute(parts[d], 'x', [(i, (i + d) % 4) for i in range(4)])]
    ppermute x2 -> x0, waiting for transfers between devices: 3.74 us -> none  [the longest x1 2.5 us: shards(): moved = lax.ppermute(placed, 'x', near)]
    ppermute x2 -> x0, starting transfers between devices: 2.64 us -> none  [the longest x1 2.56 us: shards(): other = lax.ppermute(placed, 'x', far)]
    unnamed x18, local copies, waits for them, and re-layouts: 2.15 us -> 0.12 us
    ppermute x1, waiting for transfers between devices: 1.48 us -> 0.01 us  [shards(): moved = lax.ppermute(query, 'x', far)]
    ppermute x1, waiting for transfers between devices: 1.35 us -> 0.01 us  [shards(): payload_other = lax.ppermute(payload_widening, 'c', swap)]
  transfers between devices with their start and end apart: 13 -> 10, of which waited for: 8 -> 5; matrix products, arithmetic and copies ran while one was open for 2% -> 2% of each run, Pallas kernels for 6% -> 7%
where the time goes in v3:
time: 47.6 us; the launch traced here: 47.3 us
  starting transfers between devices  18.7 us (39%)
  blocking collectives  16.1 us (34%)
  Pallas kernels  5.45 us (11%)
  waiting for transfers between devices  5.36 us (11%)
  between operations  0.73 us (2%)
  matrix products  0.49 us (1%)
    all_to_all x1, blocking collectives, exchange(): lax.all_to_all(array, SP_TP, 0, 0, tiled=True, axis_index_groups=groups)  16.1 us
    all_to_all x1, starting transfers between devices, exchange(): lax.all_to_all(array, SP_TP, 0, 0, tiled=True, axis_index_groups=groups)  9.81 us
    ppermute x3, starting transfers between devices, shards(): lax.ppermute(parts[d], 'x', [(i, (i + d) % 4) for i in range(4)])  3.88 us
    pallas_call x1, Pallas kernels, shards(): call(project_kernel, shape((seqs, pos_local // 2, 1152), BF16), 130000000...  3.1 us
    ppermute x1, starting transfers between devices, shards(): moved = lax.ppermute(query, 'x', far)  2.67 us
    ppermute x1, waiting for transfers between devices, shards(): moved = lax.ppermute(query, 'x', near)  2.53 us
    ppermute x3, waiting for transfers between devices, shards(): lax.ppermute(parts[d], 'x', [(i, (i + d) % 4) for i in range(4)])  2.36 us
    ppermute x1, starting transfers between devices, shards(): nope_other = lax.ppermute(query_nope[0], 'c', swap)  1.46 us
  transfers between devices with their start and end apart: 10, of which 5 were waited for; matrix products, arithmetic and copies ran while one was open for 2% of the time, Pallas kernels for 7%

profile of v3, /device:TPU:1, one launch (start us, length us, event | category | flops | bytes accessed | tf_op | source)
XLA Modules:
  0.0 47.3 jit_solution(15929567028608551309)
XLA Ops:
  0.6 1.5 %collective-permute-start = (bf16[2,128]{1,0:T(2,128)(2,1)}, bf16[2,128]{1,0:T(2,128)(2,1)S(1)}, u32[]{:S(2)}, u32[]{:S(2)}) collective-permute-start(bf16[2,128]{1,0:T(2,128)(2,1)} %bitcast.23), channel_id=1, source_target_pairs={{0,1},{1,0},{2,3},{3,2},{4,5},{5,4},{6,7},{7,6},{8,9},{9,8},{10,11... | collective-permute-start | bytes 1544 | tf_op jit(solution)/shard_map/ppermute | solution.py:214
  2.1 0.1 collective-permute-start.1
  2.2 0.4 collective-permute-start.4
  2.6 0.1 collective-permute-start.5
  2.7 0.1 broadcast_in_dim_tile.3.freq_ref
  2.8 0.0 copy-start.2
  2.8 0.0 copy-start.4
  2.8 0.0 copy-start.5
  2.8 0.1 shard_map.112.cs_ref
  2.9 0.4 collective-permute-done.1.qr_other_ref
  3.4 0.1 copy-done.6
  3.5 0.0 copy-done.7
  3.5 2.7 %collective-permute-start.2 = (bf16[16,256]{1,0:T(8,128)(2,1)S(1)}, bf16[16,256]{1,0:T(8,128)(2,1)S(1)}, u32[]{:S(2)}, u32[]{:S(2)}) collective-permute-start(bf16[16,256]{1,0:T(8,128)(2,1)S(1)} %shard_map.114), channel_id=1, source_target_pairs={{0,6},{6,0},{2,4},{4,2},{1,7},{7,1},{3,5},{5,3},{8,14},{14,8},{10,... | collective-permute-start | bytes 24584 | tf_op jit(solution)/shard_map/ppermute | solution.py:229
  6.2 3.1 %shard_map.113 = bf16[16,16,1152]{2,1,0:T(8,128)(2,1)} custom-call(bf16[512,2048]{1,0:T(8,128)(2,1)S(1)} %bitcast.19, f32[1,2048]{1,0:T(1,128)S(1)} %bitcast.21, bf16[2048,512]{1,0:T(8,128)(2,1)S(1)} %copy-done.1, bf16[64,2048]{1,0:T(8,128)(2,1)S(1)} %bitcast.20, f32[1,512]{1,0:T(1,128)S(1)} %bitcast.22, f32[2,32,64]{2,1,0:T(8,128)S(1)} %shard_map.112.cs_ref), custom_call_target="tpu_custom_call" | custom-call | flops 1300000000 | bytes 5000000 | tf_op jit(solution)/shard_map/pallas_call | solution.py:233
  9.3 9.8 %all-to-all-start = ((bf16[16,16,1152]{2,1,0:T(8,128)(2,1)}), bf16[16,16,1152]{2,1,0:T(8,128)(2,1)S(1)}, u32[]{:S(2)}, u32[]{:S(2)}) async-start(bf16[16,16,1152]{2,1,0:T(8,128)(2,1)} %shard_map.113), calls=%async_computation | async-start | bytes 1179648 | tf_op jit(solution)/shard_map/all_to_all | solution.py:181
  19.1 0.3 collective-permute-start.3
  19.5 2.5 %collective-permute-done.3 = bf16[16,256]{1,0:T(8,128)(2,1)S(1)} collective-permute-done((bf16[16,256]{1,0:T(8,128)(2,1)S(1)}, bf16[16,256]{1,0:T(8,128)(2,1)S(1)}, u32[]{:S(2)}, u32[]{:S(2)}) %collective-permute-start.3) | collective-permute-done | bytes 8224 | tf_op jit(solution)/shard_map/ppermute | solution.py:231
  22.0 0.1 subtract_convert_fusion
  22.1 0.2 fusion.2
  22.3 0.3 fusion
  22.6 0.1 pad_maximum_fusion.share_ref
  22.7 0.2 shard_map.115
  22.9 0.3 collective-permute-start.6
  23.2 2.4 %collective-permute-start.7 = (bf16[2,80,256]{2,1,0:T(8,128)(2,1)S(1)}, bf16[2,80,256]{2,1,0:T(8,128)(2,1)S(1)}, u32[]{:S(2)}, u32[]{:S(2)}) collective-permute-start(bf16[2,80,256]{2,1,0:T(8,128)(2,1)S(1)} %get-tuple-element.14), channel_id=1, source_target_pairs={{0,4},{2,6},{4,0},{6,2},{1,5},{3,7},{5,1},{7,3},{8,12},{10,14},{12... | collective-permute-start | bytes 245768 | tf_op jit(solution)/shard_map/ppermute | solution.py:267
  25.7 1.2 %collective-permute-start.8 = (bf16[2,80,256]{2,1,0:T(8,128)(2,1)S(1)}, bf16[2,80,256]{2,1,0:T(8,128)(2,1)S(1)}, u32[]{:S(2)}, u32[]{:S(2)}) collective-permute-start(bf16[2,80,256]{2,1,0:T(8,128)(2,1)S(1)} %get-tuple-element.15), channel_id=1, source_target_pairs={{0,6},{2,0},{4,2},{6,4},{1,7},{3,1},{5,3},{7,5},{8,14},{10,8},{12,... | collective-permute-start | bytes 245768 | tf_op jit(solution)/shard_map/ppermute | solution.py:267
  26.8 0.1 fusion.8.t_ref
  26.9 0.9 %collective-permute-done.6.p1_ref = bf16[2,80,256]{2,1,0:T(8,128)(2,1)S(1)} collective-permute-done((bf16[2,80,256]{2,1,0:T(8,128)(2,1)S(1)}, bf16[2,80,256]{2,1,0:T(8,128)(2,1)S(1)}, u32[]{:S(2)}, u32[]{:S(2)}) %collective-permute-start.6) | collective-permute-done | bytes 81952 | tf_op jit(solution)/shard_map/ppermute | solution.py:267
  27.8 0.6 %collective-permute-done.7.p2_ref = bf16[2,80,256]{2,1,0:T(8,128)(2,1)S(1)} collective-permute-done((bf16[2,80,256]{2,1,0:T(8,128)(2,1)S(1)}, bf16[2,80,256]{2,1,0:T(8,128)(2,1)S(1)}, u32[]{:S(2)}, u32[]{:S(2)}) %collective-permute-start.7) | collective-permute-done | bytes 81952 | tf_op jit(solution)/shard_map/ppermute | solution.py:267
  28.4 0.9 %collective-permute-done.8.p3_ref = bf16[2,80,256]{2,1,0:T(8,128)(2,1)S(1)} collective-permute-done((bf16[2,80,256]{2,1,0:T(8,128)(2,1)S(1)}, bf16[2,80,256]{2,1,0:T(8,128)(2,1)S(1)}, u32[]{:S(2)}, u32[]{:S(2)}) %collective-permute-start.8) | collective-permute-done | bytes 81952 | tf_op jit(solution)/shard_map/ppermute | solution.py:267
  29.3 0.6 %shard_map.116 = (bf16[8,80,512]{2,1,0:T(8,128)(2,1)S(1)}, bf16[8,64,256]{2,1,0:T(8,128)(2,1)S(1)}) custom-call(bf16[16,16,1152]{2,1,0:T(8,128)(2,1)S(1)} %all-to-all-done.z_ref, bf16[2,80,256]{2,1,0:T(8,128)(2,1)S(1)} %get-tuple-element.12.p0_ref, bf16[2,80,256]{2,1,0:T(8,128)(2,1)S(1)} %collective-permute-done.6.p1_ref, ...), custom_call_target="tpu_custom_call" | custom-call | flops 600000000 | bytes 1300000 | tf_op jit(solution)/shard_map/pallas_call | solution.py:271
  29.9 16.1 %all_to_all.10.y_ref = bf16[8,80,512]{2,1,0:T(8,128)(2,1)S(1)} all-to-all(bf16[8,80,512]{2,1,0:T(8,128)(2,1)S(1)} %get-tuple-element.16), channel_id=1, replica_groups={{7,6,5,4,3,2,1,0},{15,14,13,12,11,10,9,8},{23,22,21,20,19,18,17,16},{31..., dimensions={0} | all-to-all | bytes 1310720 | tf_op jit(solution)/shard_map/all_to_all | solution.py:181
  45.9 1.4 %shard_map.117 = (bf16[64,4096]{1,0:T(8,128)(2,1)}, bf16[8,4096]{1,0:T(8,128)(2,1)}, bf16[2,128]{1,0:T(2,128)(2,1)}) custom-call(bf16[8,80,512]{2,1,0:T(8,128)(2,1)S(1)} %all_to_all.10.y_ref, bf16[8,64,256]{2,1,0:T(8,128)(2,1)S(1)} %get-tuple-element.17.w_ref), custom_call_target="tpu_custom_call" | custom-call | flops 10000000 | bytes 1800000 | tf_op jit(solution)/shard_map/pallas_call | solution.py:280
  (27 shorter events, 0.1 us)
Async XLA Ops:
  0.6 2.8 %collective-permute-start = (bf16[2,128]{1,0:T(2,128)(2,1)}, bf16[2,128]{1,0:T(2,128)(2,1)S(1)}, u32[]{:S(2)}, u32[]{:S(2)}) collective-permute-start(bf16[2,128]{1,0:T(2,128)(2,1)} %bitcast.23), channel_id=1, source_target_pairs={{0,1},{1,0},{2,3},{3,2},{4,5},{5,4},{6,7},{7,6},{8,9},{9,8},{10,11... | collective-permute-start | bytes 1544 | tf_op jit(solution)/shard_map/ppermute | solution.py:214
  2.1 1.3 %collective-permute-start.1 = (bf16[2,64]{1,0:T(2,128)(2,1)}, bf16[2,64]{1,0:T(2,128)(2,1)S(1)}, u32[]{:S(2)}, u32[]{:S(2)}) collective-permute-start(bf16[2,64]{1,0:T(2,128)(2,1)} %bitcast.25), channel_id=1, source_target_pairs={{0,1},{1,0},{2,3},{3,2},{4,5},{5,4},{6,7},{7,6},{8,9},{9,8},{10,11... | collective-permute-start | bytes 776 | tf_op jit(solution)/shard_map/ppermute | solution.py:215
  2.2 20.1 %collective-permute-start.4 = (bf16[64,16,128]{2,1,0:T(8,128)(2,1)}, bf16[64,16,128]{2,1,0:T(8,128)(2,1)S(1)}, u32[]{:S(2)}, u32[]{:S(2)}) collective-permute-start(bf16[64,16,128]{2,1,0:T(8,128)(2,1)} %param.14), channel_id=1, source_target_pairs={{0,1},{1,0},{2,3},{3,2},{4,5},{5,4},{6,7},{7,6},{8,9},{9,8},{10,11... | collective-permute-start | bytes 786440 | tf_op jit(solution)/shard_map/ppermute | solution.py:212
  2.6 20.1 %collective-permute-start.5 = (bf16[64,16,128]{2,1,0:T(8,128)(2,1)}, bf16[64,16,128]{2,1,0:T(8,128)(2,1)S(1)}, u32[]{:S(2)}, u32[]{:S(2)}) collective-permute-start(bf16[64,16,128]{2,1,0:T(8,128)(2,1)} %own_ref.1), channel_id=1, source_target_pairs={{0,1},{1,0},{2,3},{3,2},{4,5},{5,4},{6,7},{7,6},{8,9},{9,8},{10,11... | collective-permute-start | bytes 786440 | tf_op jit(solution)/shard_map/ppermute | solution.py:213
  2.8 0.7 %copy-start.6 = (bf16[1,2,128]{2,1,0:T(2,128)(2,1)S(1)}, bf16[1,2,128]{2,1,0:T(2,128)(2,1)}, u32[]{:S(2)}) copy-start(bf16[1,2,128]{2,1,0:T(2,128)(2,1)} %param.16) | copy-start | bytes 1540
  2.8 0.7 %copy-start.7 = (bf16[1,2,64]{2,1,0:T(2,128)(2,1)S(1)}, bf16[1,2,64]{2,1,0:T(2,128)(2,1)}, u32[]{:S(2)}) copy-start(bf16[1,2,64]{2,1,0:T(2,128)(2,1)} %param.17) | copy-start | bytes 772
  2.8 3.4 %copy-start = (bf16[16,32,2048]{2,1,0:T(8,128)(2,1)S(1)}, bf16[16,32,2048]{2,1,0:T(8,128)(2,1)}, u32[]{:S(2)}) copy-start(bf16[16,32,2048]{2,1,0:T(8,128)(2,1)} %param.9) | copy-start | bytes 6291460
  2.8 3.4 %copy-start.1 = (bf16[2048,512]{1,0:T(8,128)(2,1)S(1)}, bf16[2048,512]{1,0:T(8,128)(2,1)}, u32[]{:S(2)}) copy-start(bf16[2048,512]{1,0:T(8,128)(2,1)} %w_ref.1) | copy-start | bytes 6291460
  2.8 3.4 %copy-start.2 = (bf16[2048,64]{0,1:T(8,128)(2,1)S(1)}, bf16[2048,64]{0,1:T(8,128)(2,1)}, u32[]{:S(2)}) copy-start(bf16[2048,64]{0,1:T(8,128)(2,1)} %param.12) | copy-start | bytes 786436
  2.8 3.3 %copy-start.4 = (f32[2048]{0:T(1024)S(1)}, f32[2048]{0:T(1024)}, u32[]{:S(2)}) copy-start(f32[2048]{0:T(1024)} %param.10) | copy-start | bytes 24580
  2.8 3.3 %copy-start.5 = (f32[512]{0:T(512)S(1)}, f32[512]{0:T(512)}, u32[]{:S(2)}) copy-start(f32[512]{0:T(512)} %param.13) | copy-start | bytes 6148
  3.5 15.6 %collective-permute-start.2 = (bf16[16,256]{1,0:T(8,128)(2,1)S(1)}, bf16[16,256]{1,0:T(8,128)(2,1)S(1)}, u32[]{:S(2)}, u32[]{:S(2)}) collective-permute-start(bf16[16,256]{1,0:T(8,128)(2,1)S(1)} %shard_map.114), channel_id=1, source_target_pairs={{0,6},{6,0},{2,4},{4,2},{1,7},{7,1},{3,5},{5,3},{8,14},{14,8},{10,... | collective-permute-start | bytes 24584 | tf_op jit(solution)/shard_map/ppermute | solution.py:229
  6.2 15.9 %copy-start.8 = (bf16[64,16,128]{2,1,0:T(8,128)(2,1)S(1)}, bf16[64,16,128]{2,1,0:T(8,128)(2,1)}, u32[]{:S(2)}) copy-start(bf16[64,16,128]{2,1,0:T(8,128)(2,1)} %param.14) | copy-start | bytes 786436
  9.3 13.4 %copy-start.3 = (bf16[64,16,128]{2,1,0:T(8,128)(2,1)S(1)}, bf16[64,16,128]{2,1,0:T(8,128)(2,1)}, u32[]{:S(2)}) copy-start(bf16[64,16,128]{2,1,0:T(8,128)(2,1)} %own_ref.1) | copy-start | bytes 786436
  9.3 20.0 %all-to-all-start = ((bf16[16,16,1152]{2,1,0:T(8,128)(2,1)}), bf16[16,16,1152]{2,1,0:T(8,128)(2,1)S(1)}, u32[]{:S(2)}, u32[]{:S(2)}) async-start(bf16[16,16,1152]{2,1,0:T(8,128)(2,1)} %shard_map.113), calls=%async_computation | async-start | bytes 1179648 | tf_op jit(solution)/shard_map/all_to_all | solution.py:181
  19.1 2.9 %collective-permute-start.3 = (bf16[16,256]{1,0:T(8,128)(2,1)S(1)}, bf16[16,256]{1,0:T(8,128)(2,1)S(1)}, u32[]{:S(2)}, u32[]{:S(2)}) collective-permute-start(bf16[16,256]{1,0:T(8,128)(2,1)S(1)} %add.11), channel_id=1, source_target_pairs={{0,2},{2,0},{4,6},{6,4},{1,3},{3,1},{5,7},{7,5},{8,10},{10,8},{12,... | collective-permute-start | bytes 24584 | tf_op jit(solution)/shard_map/ppermute | solution.py:231
  22.9 4.9 %collective-permute-start.6 = (bf16[2,80,256]{2,1,0:T(8,128)(2,1)S(1)}, bf16[2,80,256]{2,1,0:T(8,128)(2,1)S(1)}, u32[]{:S(2)}, u32[]{:S(2)}) collective-permute-start(bf16[2,80,256]{2,1,0:T(8,128)(2,1)S(1)} %get-tuple-element.13), channel_id=1, source_target_pairs={{0,2},{2,4},{4,6},{6,0},{1,3},{3,5},{5,7},{7,1},{8,10},{10,12},{12... | collective-permute-start | bytes 245768 | tf_op jit(solution)/shard_map/ppermute | solution.py:267
  23.2 5.2 %collective-permute-start.7 = (bf16[2,80,256]{2,1,0:T(8,128)(2,1)S(1)}, bf16[2,80,256]{2,1,0:T(8,128)(2,1)S(1)}, u32[]{:S(2)}, u32[]{:S(2)}) collective-permute-start(bf16[2,80,256]{2,1,0:T(8,128)(2,1)S(1)} %get-tuple-element.14), channel_id=1, source_target_pairs={{0,4},{2,6},{4,0},{6,2},{1,5},{3,7},{5,1},{7,3},{8,12},{10,14},{12... | collective-permute-start | bytes 245768 | tf_op jit(solution)/shard_map/ppermute | solution.py:267
  25.7 3.6 %collective-permute-start.8 = (bf16[2,80,256]{2,1,0:T(8,128)(2,1)S(1)}, bf16[2,80,256]{2,1,0:T(8,128)(2,1)S(1)}, u32[]{:S(2)}, u32[]{:S(2)}) collective-permute-start(bf16[2,80,256]{2,1,0:T(8,128)(2,1)S(1)} %get-tuple-element.15), channel_id=1, source_target_pairs={{0,6},{2,0},{4,2},{6,4},{1,7},{3,1},{5,3},{7,5},{8,14},{10,8},{12,... | collective-permute-start | bytes 245768 | tf_op jit(solution)/shard_map/ppermute | solution.py:267

commit v4 on v3

--- a/solution.py
+++ b/solution.py
@@ -62,14 +62,17 @@
     out_ref[...] = jnp.where(row == lax.axis_index("x"), rows, 0.0).astype(BF16)
 
 
-def pack_payload_kernel(share_ref, own_ref, other_ref, *refs):
+def pack_payload_kernel(mine_ref, partner_ref, own_ref, other_ref, *refs):
     x, core = lax.axis_index("x"), lax.axis_index("c")
     outs, (own_f32, other_f32) = refs[:4], refs[4:]
     each = own_ref.shape[0]
-    absorbed = jnp.concatenate([share_ref[...], jnp.zeros_like(share_ref)], axis=1)
+    mine, partner = mine_ref[...], partner_ref[...]
+    first, second = jnp.where(core == 0, mine, partner), jnp.where(core == 0, partner, mine)
+    blank = jnp.zeros((mine.shape[0], 128), F32)
+    absorbed = jnp.concatenate([first, second, blank], axis=1).astype(BF16)
     heads = own_ref.shape[1]
-    own_f32[...] = own_ref[...].astype(F32).reshape(own_f32.shape)
-    other_f32[...] = other_ref[...].astype(F32).reshape(other_f32.shape)
+    own_f32[0 : each * heads, :] = own_ref[...].astype(F32).reshape(each * heads, 128)
+    other_f32[0 : each * heads, :] = other_ref[...].astype(F32).reshape(each * heads, 128)
     for d, out_ref in enumerate(outs):
         first = 2 * (2 * ((x + d) % 4) + core)
         for r, source in enumerate((own_f32, other_f32)):
@@ -84,8 +87,8 @@
     x = x_ref[...].astype(F32)
     scale = lax.rsqrt(jnp.mean(x * x, axis=-1, keepdims=True) + norm_eps)
     gained = (x * gain_ref[...]).astype(BF16)
+    rot = lax.dot_general(r_ref[...], gained, LAST, preferred_element_type=F32).T
     lat = jnp.dot(gained, w_ref[...], preferred_element_type=F32)
-    rot = lax.dot_general(gained, r_ref[...], LAST, preferred_element_type=F32)
     lat = (lat * scale).astype(BF16).astype(F32)
     rot = (rot * scale).astype(BF16).astype(F32)
     mean = jnp.mean(lat * lat, axis=-1, keepdims=True)
@@ -207,7 +210,6 @@
     sp = lax.axis_size("sp")
     shape = jax.ShapeDtypeStruct
 
-    at = (lax.axis_index("x"), lax.axis_index("c"))
     swap = [(0, 1), (1, 0)]
     lookup_other = lax.ppermute(lookup_widening, "c", swap)
     payload_other = lax.ppermute(payload_widening, "c", swap)
@@ -248,20 +250,18 @@
     query = query + moved
     turn = query[:, 128 : 128 + QK_ROPE]
     query = query[:, :128]
-    own, partner = (
-        jnp.einsum("hd,chd->hc", query, weight, preferred_element_type=F32).astype(BF16)
+    mine, partner = (
+        jnp.einsum("hd,chd->hc", query, weight, preferred_element_type=F32)
         for weight in (lookup_widening, lookup_other)
     )
-    first, second = jnp.where(at[1] == 0, own, partner), jnp.where(at[1] == 0, partner, own)
-    share = jnp.concatenate([first, second], axis=1)
     each = payload_widening.shape[0]
     parts = call(
         pack_payload_kernel,
         [shape((2, each + 2 * tp, 256), BF16)] * 4,
         1_000_000,
         1_000_000,
-        scratch_shapes=[pltpu.VMEM((each * 2 * tp, 128), F32)] * 2,
-    )(share, payload_widening, payload_other)
+        scratch_shapes=[pltpu.VMEM(((each + 1) * 2 * tp, 128), F32)] * 2,
+    )(mine, partner, payload_widening, payload_other)
     pieces = [parts[0]]
     for d in (1, 2, 3):
         pieces.append(lax.ppermute(parts[d], "x", [(i, (i + d) % 4) for i in range(4)]))

time: 47.6 us -> 47.3 us (level)
  no operation moved by 1% of the time
where the time goes in v4:
time: 47.3 us; the launch traced here: 47 us
  starting transfers between devices  18.6 us (39%)
  blocking collectives  16.1 us (34%)
  Pallas kernels  5.38 us (11%)
  waiting for transfers between devices  5.37 us (11%)
  between operations  0.74 us (2%)
  matrix products  0.49 us (1%)
    all_to_all x1, blocking collectives, exchange(): lax.all_to_all(array, SP_TP, 0, 0, tiled=True, axis_index_groups=groups)  16.1 us
    all_to_all x1, starting transfers between devices, exchange(): lax.all_to_all(array, SP_TP, 0, 0, tiled=True, axis_index_groups=groups)  9.67 us
    ppermute x3, starting transfers between devices, shards(): lax.ppermute(parts[d], 'x', [(i, (i + d) % 4) for i in range(4)])  3.87 us
    pallas_call x1, Pallas kernels, shards(): call(project_kernel, shape((seqs, pos_local // 2, 1152), BF16), 130000000...  3.01 us
    ppermute x1, starting transfers between devices, shards(): moved = lax.ppermute(query, 'x', far)  2.67 us
    ppermute x1, waiting for transfers between devices, shards(): moved = lax.ppermute(query, 'x', near)  2.54 us
    ppermute x3, waiting for transfers between devices, shards(): lax.ppermute(parts[d], 'x', [(i, (i + d) % 4) for i in range(4)])  2.37 us
    ppermute x1, starting transfers between devices, shards(): nope_other = lax.ppermute(query_nope[0], 'c', swap)  1.46 us
  transfers between devices with their start and end apart: 10, of which 5 were waited for; matrix products, arithmetic and copies ran while one was open for 2% of the time, Pallas kernels for 7%

profile of v4, /device:TPU:1, one launch (start us, length us, event | category | flops | bytes accessed | tf_op | source)
XLA Modules:
  0.0 47.0 jit_solution(13938948608906199948)
XLA Ops:
  0.6 1.5 %collective-permute-start = (bf16[2,128]{1,0:T(2,128)(2,1)}, bf16[2,128]{1,0:T(2,128)(2,1)S(1)}, u32[]{:S(2)}, u32[]{:S(2)}) collective-permute-start(bf16[2,128]{1,0:T(2,128)(2,1)} %bitcast.25), channel_id=1, source_target_pairs={{0,1},{1,0},{2,3},{3,2},{4,5},{5,4},{6,7},{7,6},{8,9},{9,8},{10,11... | collective-permute-start | bytes 1544 | tf_op jit(solution)/shard_map/ppermute | solution.py:216
  2.1 0.1 collective-permute-start.1
  2.2 0.4 collective-permute-start.4
  2.6 0.1 collective-permute-start.5
  2.7 0.1 broadcast_in_dim_tile.3.freq_ref
  2.8 0.0 copy-start.2
  2.8 0.0 copy-start.4
  2.8 0.0 copy-start.5
  2.8 0.1 shard_map.112.cs_ref
  2.9 0.4 collective-permute-done.1.qr_other_ref
  3.4 0.1 copy-done.6
  3.5 0.0 copy-done.7
  3.5 2.7 %collective-permute-start.2 = (bf16[16,256]{1,0:T(8,128)(2,1)S(1)}, bf16[16,256]{1,0:T(8,128)(2,1)S(1)}, u32[]{:S(2)}, u32[]{:S(2)}) collective-permute-start(bf16[16,256]{1,0:T(8,128)(2,1)S(1)} %shard_map.114), channel_id=1, source_target_pairs={{0,6},{6,0},{2,4},{4,2},{1,7},{7,1},{3,5},{5,3},{8,14},{14,8},{10,... | collective-permute-start | bytes 24584 | tf_op jit(solution)/shard_map/ppermute | solution.py:231
  6.2 0.0 copy-start.8
  6.2 3.0 %shard_map.113 = bf16[16,16,1152]{2,1,0:T(8,128)(2,1)} custom-call(bf16[512,2048]{1,0:T(8,128)(2,1)S(1)} %bitcast.19, f32[1,2048]{1,0:T(1,128)S(1)} %bitcast.21, bf16[2048,512]{1,0:T(8,128)(2,1)S(1)} %copy-done.1, bf16[64,2048]{1,0:T(8,128)(2,1)S(1)} %bitcast.20, f32[1,512]{1,0:T(1,128)S(1)} %bitcast.24, f32[2,32,64]{2,1,0:T(8,128)S(1)} %shard_map.112.cs_ref), custom_call_target="tpu_custom_call" | custom-call | flops 1300000000 | bytes 5000000 | tf_op jit(solution)/shard_map/pallas_call | solution.py:235
  9.2 9.7 %all-to-all-start = ((bf16[16,16,1152]{2,1,0:T(8,128)(2,1)}), bf16[16,16,1152]{2,1,0:T(8,128)(2,1)S(1)}, u32[]{:S(2)}, u32[]{:S(2)}) async-start(bf16[16,16,1152]{2,1,0:T(8,128)(2,1)} %shard_map.113), calls=%async_computation | async-start | bytes 1179648 | tf_op jit(solution)/shard_map/all_to_all | solution.py:184
  18.9 0.3 collective-permute-start.3
  19.2 2.5 %collective-permute-done.3 = bf16[16,256]{1,0:T(8,128)(2,1)S(1)} collective-permute-done((bf16[16,256]{1,0:T(8,128)(2,1)S(1)}, bf16[16,256]{1,0:T(8,128)(2,1)S(1)}, u32[]{:S(2)}, u32[]{:S(2)}) %collective-permute-start.3) | collective-permute-done | bytes 8224 | tf_op jit(solution)/shard_map/ppermute | solution.py:233
  21.8 0.2 fusion.2
  22.0 0.1 subtract_convert_fusion
  22.1 0.3 fusion
  22.4 0.3 shard_map.115
  22.6 0.3 collective-permute-start.6
  22.9 2.4 %collective-permute-start.7 = (bf16[2,80,256]{2,1,0:T(8,128)(2,1)S(1)}, bf16[2,80,256]{2,1,0:T(8,128)(2,1)S(1)}, u32[]{:S(2)}, u32[]{:S(2)}) collective-permute-start(bf16[2,80,256]{2,1,0:T(8,128)(2,1)S(1)} %get-tuple-element.14), channel_id=1, source_target_pairs={{0,4},{2,6},{4,0},{6,2},{1,5},{3,7},{5,1},{7,3},{8,12},{10,14},{12... | collective-permute-start | bytes 245768 | tf_op jit(solution)/shard_map/ppermute | solution.py:267
  25.4 1.2 %collective-permute-start.8 = (bf16[2,80,256]{2,1,0:T(8,128)(2,1)S(1)}, bf16[2,80,256]{2,1,0:T(8,128)(2,1)S(1)}, u32[]{:S(2)}, u32[]{:S(2)}) collective-permute-start(bf16[2,80,256]{2,1,0:T(8,128)(2,1)S(1)} %get-tuple-element.15), channel_id=1, source_target_pairs={{0,6},{2,0},{4,2},{6,4},{1,7},{3,1},{5,3},{7,5},{8,14},{10,8},{12,... | collective-permute-start | bytes 245768 | tf_op jit(solution)/shard_map/ppermute | solution.py:267
  26.5 0.1 fusion.8.t_ref
  26.6 0.9 %collective-permute-done.6.p1_ref = bf16[2,80,256]{2,1,0:T(8,128)(2,1)S(1)} collective-permute-done((bf16[2,80,256]{2,1,0:T(8,128)(2,1)S(1)}, bf16[2,80,256]{2,1,0:T(8,128)(2,1)S(1)}, u32[]{:S(2)}, u32[]{:S(2)}) %collective-permute-start.6) | collective-permute-done | bytes 81952 | tf_op jit(solution)/shard_map/ppermute | solution.py:267
  27.5 0.6 %collective-permute-done.7.p2_ref = bf16[2,80,256]{2,1,0:T(8,128)(2,1)S(1)} collective-permute-done((bf16[2,80,256]{2,1,0:T(8,128)(2,1)S(1)}, bf16[2,80,256]{2,1,0:T(8,128)(2,1)S(1)}, u32[]{:S(2)}, u32[]{:S(2)}) %collective-permute-start.7) | collective-permute-done | bytes 81952 | tf_op jit(solution)/shard_map/ppermute | solution.py:267
  28.1 0.9 %collective-permute-done.8.p3_ref = bf16[2,80,256]{2,1,0:T(8,128)(2,1)S(1)} collective-permute-done((bf16[2,80,256]{2,1,0:T(8,128)(2,1)S(1)}, bf16[2,80,256]{2,1,0:T(8,128)(2,1)S(1)}, u32[]{:S(2)}, u32[]{:S(2)}) %collective-permute-start.8) | collective-permute-done | bytes 81952 | tf_op jit(solution)/shard_map/ppermute | solution.py:267
  29.0 0.6 %shard_map.116 = (bf16[8,80,512]{2,1,0:T(8,128)(2,1)S(1)}, bf16[8,64,256]{2,1,0:T(8,128)(2,1)S(1)}) custom-call(bf16[16,16,1152]{2,1,0:T(8,128)(2,1)S(1)} %all-to-all-done.z_ref, bf16[2,80,256]{2,1,0:T(8,128)(2,1)S(1)} %get-tuple-element.12.p0_ref, bf16[2,80,256]{2,1,0:T(8,128)(2,1)S(1)} %collective-permute-done.6.p1_ref, ...), custom_call_target="tpu_custom_call" | custom-call | flops 600000000 | bytes 1300000 | tf_op jit(solution)/shard_map/pallas_call | solution.py:271
  29.6 16.1 %all_to_all.10.y_ref = bf16[8,80,512]{2,1,0:T(8,128)(2,1)S(1)} all-to-all(bf16[8,80,512]{2,1,0:T(8,128)(2,1)S(1)} %get-tuple-element.16), channel_id=1, replica_groups={{7,6,5,4,3,2,1,0},{15,14,13,12,11,10,9,8},{23,22,21,20,19,18,17,16},{31..., dimensions={0} | all-to-all | bytes 1310720 | tf_op jit(solution)/shard_map/all_to_all | solution.py:184
  45.6 1.4 %shard_map.117 = (bf16[64,4096]{1,0:T(8,128)(2,1)}, bf16[8,4096]{1,0:T(8,128)(2,1)}, bf16[2,128]{1,0:T(2,128)(2,1)}) custom-call(bf16[8,80,512]{2,1,0:T(8,128)(2,1)S(1)} %all_to_all.10.y_ref, bf16[8,64,256]{2,1,0:T(8,128)(2,1)S(1)} %get-tuple-element.17.w_ref), custom_call_target="tpu_custom_call" | custom-call | flops 10000000 | bytes 1800000 | tf_op jit(solution)/shard_map/pallas_call | solution.py:280
  (25 shorter events, 0.1 us)
Async XLA Ops:
  0.6 2.8 %collective-permute-start = (bf16[2,128]{1,0:T(2,128)(2,1)}, bf16[2,128]{1,0:T(2,128)(2,1)S(1)}, u32[]{:S(2)}, u32[]{:S(2)}) collective-permute-start(bf16[2,128]{1,0:T(2,128)(2,1)} %bitcast.25), channel_id=1, source_target_pairs={{0,1},{1,0},{2,3},{3,2},{4,5},{5,4},{6,7},{7,6},{8,9},{9,8},{10,11... | collective-permute-start | bytes 1544 | tf_op jit(solution)/shard_map/ppermute | solution.py:216
  2.1 1.3 %collective-permute-start.1 = (bf16[2,64]{1,0:T(2,128)(2,1)}, bf16[2,64]{1,0:T(2,128)(2,1)S(1)}, u32[]{:S(2)}, u32[]{:S(2)}) collective-permute-start(bf16[2,64]{1,0:T(2,128)(2,1)} %bitcast.27), channel_id=1, source_target_pairs={{0,1},{1,0},{2,3},{3,2},{4,5},{5,4},{6,7},{7,6},{8,9},{9,8},{10,11... | collective-permute-start | bytes 776 | tf_op jit(solution)/shard_map/ppermute | solution.py:217
  2.2 19.9 %collective-permute-start.4 = (bf16[64,16,128]{2,1,0:T(8,128)(2,1)}, bf16[64,16,128]{2,1,0:T(8,128)(2,1)S(1)}, u32[]{:S(2)}, u32[]{:S(2)}) collective-permute-start(bf16[64,16,128]{2,1,0:T(8,128)(2,1)} %param.14), channel_id=1, source_target_pairs={{0,1},{1,0},{2,3},{3,2},{4,5},{5,4},{6,7},{7,6},{8,9},{9,8},{10,11... | collective-permute-start | bytes 786440 | tf_op jit(solution)/shard_map/ppermute | solution.py:214
  2.6 19.8 %collective-permute-start.5 = (bf16[64,16,128]{2,1,0:T(8,128)(2,1)}, bf16[64,16,128]{2,1,0:T(8,128)(2,1)S(1)}, u32[]{:S(2)}, u32[]{:S(2)}) collective-permute-start(bf16[64,16,128]{2,1,0:T(8,128)(2,1)} %own_ref.1), channel_id=1, source_target_pairs={{0,1},{1,0},{2,3},{3,2},{4,5},{5,4},{6,7},{7,6},{8,9},{9,8},{10,11... | collective-permute-start | bytes 786440 | tf_op jit(solution)/shard_map/ppermute | solution.py:215
  2.8 0.7 %copy-start.6 = (bf16[1,2,128]{2,1,0:T(2,128)(2,1)S(1)}, bf16[1,2,128]{2,1,0:T(2,128)(2,1)}, u32[]{:S(2)}) copy-start(bf16[1,2,128]{2,1,0:T(2,128)(2,1)} %param.16) | copy-start | bytes 1540
  2.8 0.7 %copy-start.7 = (bf16[1,2,64]{2,1,0:T(2,128)(2,1)S(1)}, bf16[1,2,64]{2,1,0:T(2,128)(2,1)}, u32[]{:S(2)}) copy-start(bf16[1,2,64]{2,1,0:T(2,128)(2,1)} %param.17) | copy-start | bytes 772
  2.8 3.4 %copy-start = (bf16[16,32,2048]{2,1,0:T(8,128)(2,1)S(1)}, bf16[16,32,2048]{2,1,0:T(8,128)(2,1)}, u32[]{:S(2)}) copy-start(bf16[16,32,2048]{2,1,0:T(8,128)(2,1)} %param.9) | copy-start | bytes 6291460
  2.8 3.4 %copy-start.1 = (bf16[2048,512]{1,0:T(8,128)(2,1)S(1)}, bf16[2048,512]{1,0:T(8,128)(2,1)}, u32[]{:S(2)}) copy-start(bf16[2048,512]{1,0:T(8,128)(2,1)} %w_ref.1) | copy-start | bytes 6291460
  2.8 3.4 %copy-start.2 = (bf16[2048,64]{0,1:T(8,128)(2,1)S(1)}, bf16[2048,64]{0,1:T(8,128)(2,1)}, u32[]{:S(2)}) copy-start(bf16[2048,64]{0,1:T(8,128)(2,1)} %param.12) | copy-start | bytes 786436
  2.8 3.3 %copy-start.4 = (f32[2048]{0:T(1024)S(1)}, f32[2048]{0:T(1024)}, u32[]{:S(2)}) copy-start(f32[2048]{0:T(1024)} %param.10) | copy-start | bytes 24580
  2.8 3.3 %copy-start.5 = (f32[512]{0:T(512)S(1)}, f32[512]{0:T(512)}, u32[]{:S(2)}) copy-start(f32[512]{0:T(512)} %param.13) | copy-start | bytes 6148
  3.5 15.4 %collective-permute-start.2 = (bf16[16,256]{1,0:T(8,128)(2,1)S(1)}, bf16[16,256]{1,0:T(8,128)(2,1)S(1)}, u32[]{:S(2)}, u32[]{:S(2)}) collective-permute-start(bf16[16,256]{1,0:T(8,128)(2,1)S(1)} %shard_map.114), channel_id=1, source_target_pairs={{0,6},{6,0},{2,4},{4,2},{1,7},{7,1},{3,5},{5,3},{8,14},{14,8},{10,... | collective-permute-start | bytes 24584 | tf_op jit(solution)/shard_map/ppermute | solution.py:231
  6.2 15.6 %copy-start.8 = (bf16[64,16,128]{2,1,0:T(8,128)(2,1)S(1)}, bf16[64,16,128]{2,1,0:T(8,128)(2,1)}, u32[]{:S(2)}) copy-start(bf16[64,16,128]{2,1,0:T(8,128)(2,1)} %param.14) | copy-start | bytes 786436
  6.2 16.2 %copy-start.3 = (bf16[64,16,128]{2,1,0:T(8,128)(2,1)S(1)}, bf16[64,16,128]{2,1,0:T(8,128)(2,1)}, u32[]{:S(2)}) copy-start(bf16[64,16,128]{2,1,0:T(8,128)(2,1)} %own_ref.1) | copy-start | bytes 786436
  9.2 19.8 %all-to-all-start = ((bf16[16,16,1152]{2,1,0:T(8,128)(2,1)}), bf16[16,16,1152]{2,1,0:T(8,128)(2,1)S(1)}, u32[]{:S(2)}, u32[]{:S(2)}) async-start(bf16[16,16,1152]{2,1,0:T(8,128)(2,1)} %shard_map.113), calls=%async_computation | async-start | bytes 1179648 | tf_op jit(solution)/shard_map/all_to_all | solution.py:184
  18.9 2.9 %collective-permute-start.3 = (bf16[16,256]{1,0:T(8,128)(2,1)S(1)}, bf16[16,256]{1,0:T(8,128)(2,1)S(1)}, u32[]{:S(2)}, u32[]{:S(2)}) collective-permute-start(bf16[16,256]{1,0:T(8,128)(2,1)S(1)} %add.11), channel_id=1, source_target_pairs={{0,2},{2,0},{4,6},{6,4},{1,3},{3,1},{5,7},{7,5},{8,10},{10,8},{12,... | collective-permute-start | bytes 24584 | tf_op jit(solution)/shard_map/ppermute | solution.py:233
  22.6 4.9 %collective-permute-start.6 = (bf16[2,80,256]{2,1,0:T(8,128)(2,1)S(1)}, bf16[2,80,256]{2,1,0:T(8,128)(2,1)S(1)}, u32[]{:S(2)}, u32[]{:S(2)}) collective-permute-start(bf16[2,80,256]{2,1,0:T(8,128)(2,1)S(1)} %get-tuple-element.13), channel_id=1, source_target_pairs={{0,2},{2,4},{4,6},{6,0},{1,3},{3,5},{5,7},{7,1},{8,10},{10,12},{12... | collective-permute-start | bytes 245768 | tf_op jit(solution)/shard_map/ppermute | solution.py:267
  22.9 5.2 %collective-permute-start.7 = (bf16[2,80,256]{2,1,0:T(8,128)(2,1)S(1)}, bf16[2,80,256]{2,1,0:T(8,128)(2,1)S(1)}, u32[]{:S(2)}, u32[]{:S(2)}) collective-permute-start(bf16[2,80,256]{2,1,0:T(8,128)(2,1)S(1)} %get-tuple-element.14), channel_id=1, source_target_pairs={{0,4},{2,6},{4,0},{6,2},{1,5},{3,7},{5,1},{7,3},{8,12},{10,14},{12... | collective-permute-start | bytes 245768 | tf_op jit(solution)/shard_map/ppermute | solution.py:267
  25.4 3.6 %collective-permute-start.8 = (bf16[2,80,256]{2,1,0:T(8,128)(2,1)S(1)}, bf16[2,80,256]{2,1,0:T(8,128)(2,1)S(1)}, u32[]{:S(2)}, u32[]{:S(2)}) collective-permute-start(bf16[2,80,256]{2,1,0:T(8,128)(2,1)S(1)} %get-tuple-element.15), channel_id=1, source_target_pairs={{0,6},{2,0},{4,2},{6,4},{1,7},{3,1},{5,3},{7,5},{8,14},{10,8},{12,... | collective-permute-start | bytes 245768 | tf_op jit(solution)/shard_map/ppermute | solution.py:267
